TPU v7x, 32 devices: a whole 2x2x4 slice. The times are simulated.
32 devices in a mesh: grp: 2 (over y), kv: 4 (over z), tp: 4 (over x, core).
Axes of the slice: x: 2, y: 2, z: 4, core: 2. Of those that a mesh axis runs over, the one named last changes fastest.
Arguments:
- stream: bfloat16 [256, 2048], P('grp', ('kv', 'tp')), parts along dimension 0, may hold values from -72 to 72
- lengths: int32 [256], P(('grp', 'kv')), parts along dimension 0, may hold values from 1 to 8, 384 in all
- delta_state: float32 [256, 32, 128, 128], P(('grp', 'kv'), 'tp'), parts along dimension 0, may hold values from -0.6 to 0.6
- q_hist: bfloat16 [256, 3, 2048], P(('grp', 'kv'), None, 'tp'), parts along dimension 0, may hold values from -6 to 6
- k_hist: bfloat16 [256, 3, 2048], P(('grp', 'kv'), None, 'tp'), parts along dimension 0, may hold values from -6 to 6
- v_hist: bfloat16 [256, 3, 4096], P(('grp', 'kv'), None, 'tp'), parts along dimension 0, may hold values from -6 to 6
- norm_gain: bfloat16 [2048], replicated, may hold values from 0.099609375 to 1.8984375
- w_query: bfloat16 [2048, 2048], P('kv', 'tp'), may hold values from -0.125 to 0.125
- w_key: bfloat16 [2048, 2048], P('kv', 'tp'), may hold values from -0.125 to 0.125
- w_value: bfloat16 [2048, 4096], P('kv', 'tp'), may hold values from -0.125 to 0.125
- w_gate: bfloat16 [2048, 4096], P('kv', 'tp'), may hold values from -0.125 to 0.125
- w_beta: bfloat16 [2048, 32], replicated, may hold values from -0.125 to 0.125
- w_decay: bfloat16 [2048, 32], replicated, may hold values from -0.125 to 0.125
- conv_query: bfloat16 [4, 2048], replicated, may hold values from -3 to 3
- conv_key: bfloat16 [4, 2048], replicated, may hold values from -3 to 3
- conv_value: bfloat16 [4, 4096], replicated, may hold values from -3 to 3
- decay_log: float32 [32], replicated, may hold values from 0 to 2.77
- time_bias: float32 [32], replicated, may hold values from -4 to 0
- out_gain: bfloat16 [128], replicated, may hold values from 0.099609375 to 1.8984375
- w_out: bfloat16 [4096, 2048], P('tp', 'kv'), may hold values from -0.09375 to 0.09375
- mlp_gain: bfloat16 [2048], replicated, may hold values from 0.099609375 to 1.8984375
- w_up: bfloat16 [2048, 8192], P('kv', 'tp'), may hold values from -0.125 to 0.125
- w_down: bfloat16 [8192, 2048], P('tp', 'kv'), may hold values from -0.0625 to 0.0625
Outputs:
- result: bfloat16 [256, 2048], P('grp', ('kv', 'tp')), parts along dimension 0
- new_state: float32 [256, 32, 128, 128], P(('grp', 'kv'), 'tp'), parts along dimension 0
There are 2 independent parts, one for each index of `grp`. A program takes and returns all parts, laid end to end along the dimension named above; an argument that names none is the same for every part. Nothing has to cross between parts.
All inputs are finite; a program needn't handle non-finite values. No bound on the sum of `lengths` on one device may be relied on, other than what follows from the above.
Results may differ from a plain program's by a relative error of at most 0.01.
Values may be sent and summed in bfloat16 or wider, within the bound.
A program may use at most 128 MiB of HBM per device.

v0:
```python
import functools

import jax
import jax.numpy as jnp
from jax import lax
from jax.experimental import pallas as pl
from jax.experimental.pallas import tpu as pltpu
from jax.sharding import PartitionSpec as P

EPSILON = 1e-06
MESH = pl.DeviceIdType.MESH
F32 = jnp.float32
BF16 = jnp.bfloat16
LANES = 128


def greet(axes):
    barrier = pltpu.get_barrier_semaphore()
    total = 0
    for name, size in axes:
        me = lax.axis_index(name)
        for step in range(1, size):
            pl.semaphore_signal(
                barrier, inc=1, device_id={name: lax.rem(me + step, size)}, device_id_type=MESH
            )
            total += 1
    pl.semaphore_wait(barrier, total)


def order(size):
    return sorted(range(1, size), key=lambda step: -min(step, size - step))


def scatter_copies(name, size, src, dst, send, recv):
    me = lax.axis_index(name)
    copies = []
    for step in order(size):
        peer = lax.rem(me + step, size)
        copies.append(
            pltpu.make_async_remote_copy(
                src_ref=src.at[peer],
                dst_ref=dst.at[step - 1],
                send_sem=send.at[step - 1],
                recv_sem=recv.at[step - 1],
                device_id={name: peer},
                device_id_type=MESH,
            )
        )
    return copies


def gather_copies(name, size, src, dst, send, recv):
    me = lax.axis_index(name)
    copies = []
    for step in order(size):
        peer = lax.rem(me + step, size)
        copies.append(
            pltpu.make_async_remote_copy(
                src_ref=src,
                dst_ref=dst.at[me],
                send_sem=send.at[step - 1],
                recv_sem=recv.at[step - 1],
                device_id={name: peer},
                device_id_type=MESH,
            )
        )
    return copies


def start(copies):
    for copy in copies:
        copy.start()


def wait_recv(copies):
    for copy in copies:
        copy.wait_recv()


def wait_send(copies):
    for copy in copies:
        copy.wait_send()


def silu(values):
    return values * jax.nn.sigmoid(values)


def softplus(values):
    return jnp.maximum(values, 0.0) + jnp.log1p(jnp.exp(-jnp.abs(values)))


def row_blocks(name, columns):
    return pl.ds(pl.multiple_of(lax.axis_index(name) * columns, LANES), columns)


def project_kernel(
    n_kv, n_tp, width, head, heads_own,
    stream, lengths, gain, conv_q, conv_k, conv_v, head_params,
    q_hist, k_hist, v_hist, w_q, w_k, w_v, w_g, w_b, w_d,
    out_q, out_k, out_v, out_g, out_s, out_f,
    wq_v, wk_v, wv_v, wg_v, wb_v, wd_v, streams,
    part_q, part_k, part_v, part_g, part_e,
    got_q, got_k, got_v, got_g, got_e,
    hist_q, hist_k, hist_v, stream_v, convq_v, convk_v, convv_v,
    load_sem, hist_sem, early_sem, s_send, s_recv, p_send, p_recv,
):
    kv = lax.axis_index("kv")
    tp = lax.axis_index("tp")
    block = w_q.shape[0]
    rows = stream.shape[0]
    own = rows // n_kv
    heads_all = w_b.shape[0]
    early = pltpu.make_async_copy(stream, stream_v, early_sem)
    early.start()
    block_cols = row_blocks("kv", block)
    loads = [
        pltpu.make_async_copy(w_b.at[:, block_cols], wb_v, load_sem.at[4]),
        pltpu.make_async_copy(w_d.at[:, block_cols], wd_v, load_sem.at[5]),
        pltpu.make_async_copy(w_q, wq_v, load_sem.at[0]),
        pltpu.make_async_copy(w_k, wk_v, load_sem.at[1]),
        pltpu.make_async_copy(w_v, wv_v, load_sem.at[2]),
        pltpu.make_async_copy(w_g, wg_v, load_sem.at[3]),
        pltpu.make_async_copy(q_hist, hist_q, hist_sem.at[0]),
        pltpu.make_async_copy(k_hist, hist_k, hist_sem.at[1]),
        pltpu.make_async_copy(v_hist, hist_v, hist_sem.at[2]),
        pltpu.make_async_copy(conv_q.at[:, row_blocks("tp", convq_v.shape[1])], convq_v, hist_sem.at[3]),
        pltpu.make_async_copy(conv_k.at[:, row_blocks("tp", convk_v.shape[1])], convk_v, hist_sem.at[4]),
        pltpu.make_async_copy(conv_v.at[:, row_blocks("tp", convv_v.shape[1])], convv_v, hist_sem.at[5]),
    ]
    start(loads)
    greet((("kv", n_kv), ("tp", n_tp)))
    early.wait()
    stream_copies = gather_copies("tp", n_tp, stream_v, streams, s_send, s_recv)
    start(stream_copies)
    streams[tp] = stream_v[...]
    wait_recv(stream_copies)

    wide = jnp.concatenate([streams[t] for t in range(n_tp)], axis=1).astype(F32)
    scaled = (wide * gain[:, row_blocks("kv", block)].astype(F32)).astype(BF16)
    squares = jnp.sum(wide * wide, axis=1, keepdims=True)

    all_copies = []

    def send(index, part, got):
        copies = scatter_copies("kv", n_kv, part, got, p_send.at[index], p_recv.at[index])
        start(copies)
        all_copies.append(copies)

    loads[0].wait()
    loads[1].wait()
    contract = (((1,), (1,)), ((), ()))
    beta = lax.dot_general(scaled, wb_v[...], contract, preferred_element_type=F32)
    decay = lax.dot_general(scaled, wd_v[...], contract, preferred_element_type=F32)
    part_e[...] = jnp.concatenate(
        [beta, decay, jnp.broadcast_to(squares, (rows, LANES - 2 * heads_all))], axis=1
    ).reshape(n_kv, own, LANES)
    send(0, part_e, got_e)
    pieces = ((wq_v, part_q, got_q), (wk_v, part_k, got_k), (wv_v, part_v, got_v), (wg_v, part_g, got_g))
    for index, (weight, part, got) in enumerate(pieces):
        loads[2 + index].wait()
        product = jnp.dot(scaled, weight[...], preferred_element_type=F32)
        part[...] = product.reshape(n_kv, own, product.shape[1]).astype(BF16)
        send(1 + index, part, got)

    length = lengths[...]

    def history(hist, taps):
        total = None
        taps_count = taps.shape[0]
        for r in range(taps_count - 1):
            live = length[:, :1] >= taps_count - r
            term = jnp.where(live, hist[r].astype(F32) * taps[r : r + 1, :], 0.0)
            total = term if total is None else total + term
        return total

    for copy in loads[6:]:
        copy.wait()
    taps_q = convq_v[...].astype(F32)
    taps_k = convk_v[...].astype(F32)
    taps_v = convv_v[...].astype(F32)
    past_q = history(hist_q, taps_q)
    past_k = history(hist_k, taps_k)
    past_v = history(hist_v, taps_v)

    def collect(index, part, got):
        wait_recv(all_copies[index])
        total = part[kv].astype(F32)
        for slot in range(n_kv - 1):
            total = total + got[slot].astype(F32)
        return total

    extra = collect(0, part_e, got_e)
    row_scale = lax.rsqrt(extra[:, 2 * heads_all : 2 * heads_all + 1] / width + EPSILON)
    terms = extra * row_scale
    shift = tp * heads_own
    own_beta = pltpu.roll(terms, lax.rem(LANES - shift, LANES), 1)
    own_decay = pltpu.roll(terms, lax.rem(2 * LANES - heads_all - shift, LANES), 1)
    own_params = pltpu.roll(head_params[...], lax.rem(LANES - shift, LANES), 1)
    fade = jnp.exp(-jnp.exp(own_params[0:1, :]) * softplus(own_decay + own_params[1:2, :]))
    out_s[...] = jax.nn.sigmoid(own_beta)
    out_f[...] = jnp.where(length == 1, 0.0, fade)

    def unit(values, out, factor):
        for h in range(values.shape[1] // head):
            one = values[:, h * head : (h + 1) * head]
            scale = lax.rsqrt(jnp.sum(one * one, axis=1, keepdims=True) + EPSILON)
            out[:, h * head : (h + 1) * head] = one * (scale * factor)

    last = taps_q.shape[0] - 1
    raw_q = collect(1, part_q, got_q) * row_scale
    unit(silu(raw_q * taps_q[last : last + 1] + past_q), out_q, head ** (-0.5))
    raw_k = collect(2, part_k, got_k) * row_scale
    unit(silu(raw_k * taps_k[last : last + 1] + past_k), out_k, 1.0)
    raw_v = collect(3, part_v, got_v) * row_scale
    out_v[...] = silu(raw_v * taps_v[last : last + 1] + past_v)
    raw_g = collect(4, part_g, got_g) * row_scale
    out_g[...] = silu(raw_g)
    wait_send(stream_copies)
    for copies in all_copies:
        wait_send(copies)


def state_kernel(
    seqs, head, repeat,
    queries, keys, values, gates, gain, strength, fade, state,
    new_state, gated,
    readouts,
):
    base = pl.program_id(0) * seqs
    key_heads = keys.shape[1] // head

    @pl.loop(0, key_heads)
    def _(h):
        columns = pl.ds(pl.multiple_of(h * head, LANES), head)
        keys_t = keys[:, columns].T
        queries_t = queries[:, columns].T
        for s in range(seqs):
            key = jnp.broadcast_to(keys_t[:, s : s + 1], (head, head))
            query = jnp.broadcast_to(queries_t[:, s : s + 1], (head, head))
            for j in range(repeat):
                v = h * repeat + j
                wide = pl.ds(pl.multiple_of(v * head, LANES), head)
                carried = state[s, v] * fade[base + s, v]
                recalled = jnp.sum(carried * key, axis=0, keepdims=True)
                update = strength[base + s, v] * (values[s : s + 1, wide] - recalled)
                fresh = carried + key * update
                new_state[s, v] = fresh
                readouts[s : s + 1, wide] = jnp.sum(fresh * query, axis=0, keepdims=True)

    gain_row = gain[...].astype(F32)
    for v in range(key_heads * repeat):
        span = slice(v * head, (v + 1) * head)
        one = readouts[:, span]
        normed = one * lax.rsqrt(jnp.mean(one * one, axis=1, keepdims=True) + EPSILON)
        gated[:, span] = normed * gain_row * gates[:, span]


def mlp_kernel(
    n_kv, n_tp, width, pieces,
    gated, stream, gain, w_out, w_up, w_down,
    result,
    wo_v, wu_v, wd_v, mine, gathered, mix_part, mix_got, mixed, blocks,
    up_part, up_got, sq_part, sq_got, hidden, hiddens, down_part, down_got,
    load_sem, g_send, g_recv, m_send, m_recv, b_send, b_recv,
    q_send, q_recv, u_send, u_recv, h_send, h_recv, d_send, d_recv,
):
    kv = lax.axis_index("kv")
    tp = lax.axis_index("tp")
    rows, own_cols = stream.shape
    own = rows // n_kv
    block = w_up.shape[0]
    units = w_up.shape[1]
    piece = units // pieces
    loads = [
        pltpu.make_async_copy(w_out, wo_v, load_sem.at[0]),
        pltpu.make_async_copy(w_up, wu_v, load_sem.at[1]),
        pltpu.make_async_copy(w_down, wd_v, load_sem.at[2]),
    ]
    start(loads)
    mine[...] = gated[...].astype(BF16)
    greet((("kv", n_kv), ("tp", n_tp)))
    gated_copies = gather_copies("kv", n_kv, mine, gathered, g_send, g_recv)
    start(gated_copies)
    gathered[kv] = mine[...]
    loads[0].wait()
    wait_recv(gated_copies)

    def reduce_tp(product, part, got, send_sem, recv_sem):
        for t in range(n_tp):
            part[t] = product[:, t * own_cols : (t + 1) * own_cols].astype(BF16)
        copies = scatter_copies("tp", n_tp, part, got, send_sem, recv_sem)
        start(copies)
        wait_recv(copies)
        total = part[tp].astype(F32)
        for slot in range(n_tp - 1):
            total = total + got[slot].astype(F32)
        return total, copies

    everyone = gathered[...].reshape(rows, gathered.shape[2])
    product = jnp.dot(everyone, wo_v[...], preferred_element_type=F32)
    total, mix_copies = reduce_tp(product, mix_part, mix_got, m_send, m_recv)
    mixed_own = (stream[...].astype(F32) + total).astype(BF16)
    mixed[...] = mixed_own
    block_copies = gather_copies("tp", n_tp, mixed, blocks, b_send, b_recv)
    start(block_copies)
    blocks[tp] = mixed_own
    wait_recv(block_copies)
    wide = jnp.concatenate([blocks[t] for t in range(n_tp)], axis=1).astype(F32)
    scaled = (wide * gain[:, row_blocks("kv", block)].astype(F32)).astype(BF16)
    squares = jnp.sum(wide * wide, axis=1, keepdims=True)
    sq_part[...] = jnp.broadcast_to(squares, (rows, LANES)).reshape(n_kv, own, LANES)
    square_copies = scatter_copies("kv", n_kv, sq_part, sq_got, q_send, q_recv)
    start(square_copies)
    loads[1].wait()
    up_copies = []
    for p in range(pieces):
        product = jnp.dot(
            scaled, wu_v[:, p * piece : (p + 1) * piece], preferred_element_type=F32
        )
        up_part[p] = product.reshape(n_kv, own, piece).astype(BF16)
        copies = scatter_copies("kv", n_kv, up_part.at[p], up_got.at[p], u_send.at[p], u_recv.at[p])
        start(copies)
        up_copies.append(copies)
    wait_recv(square_copies)
    square_sum = sq_part[kv]
    for slot in range(n_kv - 1):
        square_sum = square_sum + sq_got[slot]
    unit_scale = lax.rsqrt(square_sum[:, :1] / width + EPSILON)
    hidden_copies = []
    for p in range(pieces):
        wait_recv(up_copies[p])
        total = up_part[p, kv].astype(F32)
        for slot in range(n_kv - 1):
            total = total + up_got[p, slot].astype(F32)
        active = jnp.maximum(total * unit_scale, 0.0)
        active = (active * active).astype(BF16)
        hidden[p] = active
        copies = gather_copies("kv", n_kv, hidden.at[p], hiddens.at[p], h_send.at[p], h_recv.at[p])
        start(copies)
        hiddens[p, kv] = active
        hidden_copies.append(copies)
    loads[2].wait()
    product = jnp.zeros((rows, wd_v.shape[1]), F32)
    for p in range(pieces):
        wait_recv(hidden_copies[p])
        product = product + jnp.dot(
            hiddens[p].reshape(rows, piece),
            wd_v[p * piece : (p + 1) * piece, :],
            preferred_element_type=F32,
        )
    total, down_copies = reduce_tp(product, down_part, down_got, d_send, d_recv)
    result[...] = (mixed[...].astype(F32) + total).astype(BF16)
    wait_send(gated_copies)
    wait_send(mix_copies)
    wait_send(block_copies)
    wait_send(square_copies)
    for copies in up_copies + hidden_copies:
        wait_send(copies)
    wait_send(down_copies)


def on_device(
    n_kv, n_tp,
    stream, lengths, delta_state, q_hist, k_hist, v_hist, norm_gain,
    w_query, w_key, w_value, w_gate, w_beta, w_decay,
    conv_query, conv_key, conv_value, decay_log, time_bias, out_gain,
    w_out, mlp_gain, w_up, w_down,
):
    width = norm_gain.shape[0]
    rows, own_cols = stream.shape
    own, heads_own, head = delta_state.shape[:3]
    key_cols = q_hist.shape[2]
    value_cols = v_hist.shape[2]
    block = w_query.shape[0]
    heads_all = w_beta.shape[1]
    key_heads = key_cols // head
    repeat = heads_own // key_heads
    units = w_up.shape[1]
    vmem = pl.BlockSpec(memory_space=pltpu.VMEM)
    hbm = pl.BlockSpec(memory_space=pltpu.HBM)
    dma = pltpu.SemaphoreType.DMA

    def shape(*dims, dtype=F32):
        return jax.ShapeDtypeStruct(dims, dtype)

    wide_lengths = jnp.broadcast_to(lengths[:, None], (own, LANES))
    head_params = jnp.pad(jnp.stack([decay_log, time_bias]), ((0, 6), (0, LANES - heads_all)))
    cols = (key_cols, key_cols, value_cols, value_cols)
    queries, keys, values, gates, strength, fade = pl.pallas_call(
        functools.partial(project_kernel, n_kv, n_tp, width, head, heads_own),
        out_shape=tuple(shape(own, c) for c in cols) + (shape(own, LANES), shape(own, LANES)),
        in_specs=[hbm, vmem, vmem, hbm, hbm, hbm, vmem] + [hbm] * 9,
        out_specs=(vmem,) * 6,
        scratch_shapes=[
            *(pltpu.VMEM((block, c), BF16) for c in cols),
            pltpu.VMEM((heads_all, block), BF16),
            pltpu.VMEM((heads_all, block), BF16),
            pltpu.VMEM((n_tp, rows, own_cols), BF16),
            *(pltpu.VMEM((n_kv, own, c), BF16) for c in cols),
            pltpu.VMEM((n_kv, own, LANES), F32),
            *(pltpu.VMEM((n_kv - 1, own, c), BF16) for c in cols),
            pltpu.VMEM((n_kv - 1, own, LANES), F32),
            *(pltpu.VMEM((q_hist.shape[1], own, c), BF16) for c in cols[:3]),
            pltpu.VMEM((rows, own_cols), BF16),
            *(pltpu.VMEM((conv_query.shape[0], c), BF16) for c in cols[:3]),
            dma((6,)), dma((6,)), dma(()),
            dma((n_tp - 1,)), dma((n_tp - 1,)),
            dma((5, n_kv - 1)), dma((5, n_kv - 1)),
        ],
        compiler_params=pltpu.CompilerParams(
            collective_id=0, has_side_effects=True, vmem_limit_bytes=67043328
        ),
        name="project",
    )(
        stream, wide_lengths, norm_gain[None], conv_query, conv_key, conv_value, head_params,
        *(jnp.transpose(hist, (1, 0, 2)) for hist in (q_hist, k_hist, v_hist)),
        w_query, w_key, w_value, w_gate, w_beta.T, w_decay.T,
    )

    seqs = min(8, own)
    smem = pl.BlockSpec(memory_space=pltpu.SMEM)

    def by_rows(columns):
        return pl.BlockSpec((seqs, columns), lambda i: (i, 0))

    state_spec = pl.BlockSpec((seqs, heads_own, head, head), lambda i: (i, 0, 0, 0))
    new_state, gated = pl.pallas_call(
        functools.partial(state_kernel, seqs, head, repeat),
        out_shape=(shape(*delta_state.shape), shape(own, value_cols)),
        grid=(own // seqs,),
        in_specs=[
            by_rows(key_cols), by_rows(key_cols), by_rows(value_cols), by_rows(value_cols),
            pl.BlockSpec((1, head), lambda i: (0, 0)), smem, smem, state_spec,
        ],
        out_specs=(state_spec, by_rows(value_cols)),
        scratch_shapes=[pltpu.VMEM((seqs, value_cols), F32)],
        compiler_params=pltpu.CompilerParams(vmem_limit_bytes=67043328),
        name="state",
    )(queries, keys, values, gates, out_gain[None], strength, fade, delta_state)

    pieces = 4
    piece = units // pieces
    result = pl.pallas_call(
        functools.partial(mlp_kernel, n_kv, n_tp, width, pieces),
        out_shape=shape(rows, own_cols, dtype=BF16),
        in_specs=[vmem] * 3 + [hbm] * 3,
        out_specs=vmem,
        scratch_shapes=[
            pltpu.VMEM(w_out.shape, BF16),
            pltpu.VMEM(w_up.shape, BF16),
            pltpu.VMEM(w_down.shape, BF16),
            pltpu.VMEM((own, value_cols), BF16),
            pltpu.VMEM((n_kv, own, value_cols), BF16),
            pltpu.VMEM((n_tp, rows, own_cols), BF16),
            pltpu.VMEM((n_tp - 1, rows, own_cols), BF16),
            pltpu.VMEM((rows, own_cols), BF16),
            pltpu.VMEM((n_tp, rows, own_cols), BF16),
            pltpu.VMEM((pieces, n_kv, own, piece), BF16),
            pltpu.VMEM((pieces, n_kv - 1, own, piece), BF16),
            pltpu.VMEM((n_kv, own, LANES), F32),
            pltpu.VMEM((n_kv - 1, own, LANES), F32),
            pltpu.VMEM((pieces, own, piece), BF16),
            pltpu.VMEM((pieces, n_kv, own, piece), BF16),
            pltpu.VMEM((n_tp, rows, own_cols), BF16),
            pltpu.VMEM((n_tp - 1, rows, own_cols), BF16),
            dma((3,)),
            dma((n_kv - 1,)), dma((n_kv - 1,)),
            dma((n_tp - 1,)), dma((n_tp - 1,)),
            dma((n_tp - 1,)), dma((n_tp - 1,)),
            dma((n_kv - 1,)), dma((n_kv - 1,)),
            dma((pieces, n_kv - 1)), dma((pieces, n_kv - 1)),
            dma((pieces, n_kv - 1)), dma((pieces, n_kv - 1)),
            dma((n_tp - 1,)), dma((n_tp - 1,)),
        ],
        compiler_params=pltpu.CompilerParams(
            collective_id=1, has_side_effects=True, vmem_limit_bytes=40 * 2**20
        ),
        name="mlp",
    )(gated, stream, mlp_gain[None], w_out, w_up, w_down)
    return result, new_state


def solution(mesh):
    in_specs = (
        P("grp", ("kv", "tp")),
        P(("grp", "kv")),
        P(("grp", "kv"), "tp", None, None),
        P(("grp", "kv"), None, "tp"),
        P(("grp", "kv"), None, "tp"),
        P(("grp", "kv"), None, "tp"),
        P(),
        P("kv", "tp"),
        P("kv", "tp"),
        P("kv", "tp"),
        P("kv", "tp"),
        P(),
        P(),
        P(),
        P(),
        P(),
        P(),
        P(),
        P(),
        P("tp", "kv"),
        P(),
        P("kv", "tp"),
        P("tp", "kv"),
    )
    out_specs = (P("grp", ("kv", "tp")), P(("grp", "kv"), "tp", None, None))
    return jax.shard_map(
        functools.partial(on_device, mesh.shape["kv"], mesh.shape["tp"]),
        mesh=mesh, in_specs=in_specs, out_specs=out_specs, check_vma=False,
    )
```

profile of v0, /device:TPU:0, one launch (start us, length us, event | category | flops | bytes accessed | tf_op | source)
XLA Modules:
  0.0 103.2 jit_solution(13282886869954681383)
XLA Ops:
  0.6 1.3 %broadcast_in_dim.15.lengths = s32[32,128]{1,0:T(8,128)} broadcast(s32[32]{0:T(128)} %param.24), dimensions={0} | broadcast | bytes 16512 | tf_op jit(solution)/shard_map/broadcast_in_dim | solution.py:387
  2.0 1.3 %broadcast_in_dim.16.gain = bf16[1,2048]{1,0:T(2,128)(2,1)} reshape(bf16[2048]{0:T(1024)(128)(2,1)} %param.29) | data formatting | bytes 8192 | tf_op jit(solution)/shard_map/broadcast_in_dim | solution.py:416
  3.3 1.3 %select_maximum_fusion.head_params = f32[8,128]{1,0:T(8,128)} fusion(f32[1,32]{1,0:T(1,128)} %bitcast.14, f32[1,32]{1,0:T(1,128)} %bitcast.15), kind=kLoop, calls=%fused_computation | loop fusion | flops 8192 | bytes 4352 | tf_op jit(solution)/shard_map/stack | solution.py:388
  4.5 29.9 %project.1 = (f32[32,512]{1,0:T(8,128)}, f32[32,512]{1,0:T(8,128)}, f32[32,1024]{1,0:T(8,128)}, f32[32,1024]{1,0:T(8,128)}, f32[32,128]{1,0:T(8,128)}, /*index=5*/f32[32,128]{1,0:T(8,128)}) custom-call(bf16[128,128]{1,0:T(8,128)(2,1)} %stream.3, s32[32,128]{1,0:T(8,128)} %broadcast_in_dim.15.lengths, bf16[1,2048]{1,0:T(2,128)(2,1)} %broadcast_in_dim.16.gain, ...), custom_call_target="tpu_custom_call" | custom-call | tf_op jit(solution)/shard_map/project/pallas_call | solution.py:390
  34.4 16.1 %state.2 = (f32[32,8,128,128]{3,2,1,0:T(8,128)}, f32[32,1024]{1,0:T(8,128)}) custom-call(f32[32,512]{1,0:T(8,128)} %get-tuple-element.10.queries, f32[32,512]{1,0:T(8,128)} %get-tuple-element.11.keys, f32[32,1024]{1,0:T(8,128)} %get-tuple-element.12.values, f32[32,1024]{1,0:T(8,128)} %get-tuple-element.13.gates, bf16[1,128]{1,0:T(2,128)(2,1)} %bitcast.13, ...), custom_call_target="tpu_custom_call" | custom-call | tf_op jit(solution)/shard_map/state/pallas_call | solution.py:428
  50.5 0.7 broadcast_in_dim.18.gain
  51.2 0.0 copy-start
  51.2 1.6 %copy-done = bf16[512,2048]{1,0:T(8,128)(2,1)S(1)} copy-done((bf16[512,2048]{1,0:T(8,128)(2,1)S(1)}, bf16[512,2048]{1,0:T(8,128)(2,1)}, u32[]{:S(2)}) %copy-start) | copy-done | bytes 2097176
  52.8 0.0 copy-start.1
  52.8 1.6 %copy-done.1 = bf16[2048,512]{1,0:T(8,128)(2,1)S(1)} copy-done((bf16[2048,512]{1,0:T(8,128)(2,1)S(1)}, bf16[2048,512]{1,0:T(8,128)(2,1)}, u32[]{:S(2)}) %copy-start.1) | copy-done | bytes 2097176
  54.4 0.0 copy-start.2
  54.4 1.2 %copy-done.2 = bf16[1024,512]{1,0:T(8,128)(2,1)S(1)} copy-done((bf16[1024,512]{1,0:T(8,128)(2,1)S(1)}, bf16[1024,512]{1,0:T(8,128)(2,1)}, u32[]{:S(2)}) %copy-start.2) | copy-done | bytes 1048600
  55.6 0.0 copy-start.3
  55.6 0.8 copy-done.3
  56.4 0.0 copy-start.4
  56.4 0.9 copy-done.4
  57.3 45.3 %mlp.1 = bf16[128,128]{1,0:T(8,128)(2,1)S(1)} custom-call(f32[32,1024]{1,0:T(8,128)S(1)} %copy-done.4, bf16[128,128]{1,0:T(8,128)(2,1)S(1)} %copy-done.3, bf16[1,2048]{1,0:T(2,128)(2,1)S(1)} %broadcast_in_dim.18.gain, bf16[1024,512]{1,0:T(8,128)(2,1)S(1)} %copy-done.2, bf16[512,2048]{1,0:T(8,128)(2,1)S(1)} %copy-done, bf16[2048,512]{1,0:T(8,128)(2,1)S(1)} %copy-done.1), custom_call_target="tpu_custom_call" | custom-call | tf_op jit(solution)/shard_map/mlp/pallas_call | solution.py:444
  102.6 0.6 copy.26
Async XLA Ops:
  51.2 1.6 %copy-start = (bf16[512,2048]{1,0:T(8,128)(2,1)S(1)}, bf16[512,2048]{1,0:T(8,128)(2,1)}, u32[]{:S(2)}) copy-start(bf16[512,2048]{1,0:T(8,128)(2,1)} %w_up.1) | copy-start | bytes 6291460
  52.8 1.6 %copy-start.1 = (bf16[2048,512]{1,0:T(8,128)(2,1)S(1)}, bf16[2048,512]{1,0:T(8,128)(2,1)}, u32[]{:S(2)}) copy-start(bf16[2048,512]{1,0:T(8,128)(2,1)} %w_down.1) | copy-start | bytes 6291460
  54.4 1.2 %copy-start.2 = (bf16[1024,512]{1,0:T(8,128)(2,1)S(1)}, bf16[1024,512]{1,0:T(8,128)(2,1)}, u32[]{:S(2)}) copy-start(bf16[1024,512]{1,0:T(8,128)(2,1)} %w_out.1) | copy-start | bytes 3145732
  55.6 0.8 copy-start.3
  56.4 0.9 copy-start.4
where the time goes:
time: 104 us; the launch traced here: 103 us
  Pallas kernels  91.3 us (88%)
  local copies, waits for them, and re-layouts  10 us (10%)
  other arithmetic  1.27 us (1%)
    pallas_call x1, Pallas kernels, on_device(): pl.pallas_call(functools.partial(mlp_kernel, n_kv, n_tp, width, pieces),...  45.3 us
    pallas_call x1, Pallas kernels, on_device(): pl.pallas_call(functools.partial(project_kernel, n_kv, n_tp, width, head,...  29.9 us
    pallas_call x1, Pallas kernels, on_device(): pl.pallas_call(functools.partial(state_kernel, seqs, head, repeat), out_s...  16.1 us
    unnamed x11, local copies, waits for them, and re-layouts  6.68 us

commit v1 on v0

v1 whole, which is shorter than its diff:
```python
import functools

import jax
import jax.numpy as jnp
from jax import lax
from jax.experimental import pallas as pl
from jax.experimental.pallas import tpu as pltpu
from jax.sharding import PartitionSpec as P

EPSILON = 1e-06
MESH = pl.DeviceIdType.MESH
F32 = jnp.float32
BF16 = jnp.bfloat16
LANES = 128
CONTRACT_LAST = (((1,), (1,)), ((), ()))


def greet(axes):
    barrier = pltpu.get_barrier_semaphore()
    total = 0
    for name, size in axes:
        me = lax.axis_index(name)
        for step in range(1, size):
            pl.semaphore_signal(
                barrier, inc=1, device_id={name: lax.rem(me + step, size)}, device_id_type=MESH
            )
            total += 1
    pl.semaphore_wait(barrier, total)


def order(size):
    return sorted(range(1, size), key=lambda step: -min(step, size - step))


def remote(name, peer, src, dst, send, recv):
    return pltpu.make_async_remote_copy(
        src_ref=src, dst_ref=dst, send_sem=send, recv_sem=recv,
        device_id={name: peer}, device_id_type=MESH,
    )


def scatter_copies(name, size, src, dst, send, recv):
    me = lax.axis_index(name)
    copies = []
    for step in order(size):
        peer = lax.rem(me + step, size)
        copies.append(
            remote(name, peer, src.at[peer], dst.at[step - 1], send.at[step - 1], recv.at[step - 1])
        )
    return copies


def gather_copies(name, size, src, dst, send, recv):
    me = lax.axis_index(name)
    copies = []
    for step in order(size):
        peer = lax.rem(me + step, size)
        copies.append(
            remote(name, peer, src, dst.at[me], send.at[step - 1], recv.at[step - 1])
        )
    return copies


def start(copies):
    for copy in copies:
        copy.start()


def wait_recv(copies):
    for copy in copies:
        copy.wait_recv()


def wait_send(copies):
    for copy in copies:
        copy.wait_send()


def unless(conditions, action):
    if not conditions:
        action()
        return
    skip = functools.reduce(jnp.logical_or, conditions)
    pl.when(jnp.logical_not(skip))(action)


class LineScatter:
    def __init__(self, name, size, part, got, relay_in, relay_out, send, recv, relay_recv):
        self.name, self.size, self.me = name, size, lax.axis_index(name)
        self.part, self.got = part, got
        self.relay_in, self.relay_out = relay_in, relay_out
        self.send, self.recv, self.relay_recv = send, recv, relay_recv
        self.relays = size >= 4

    def copy(self, c, step, src=None):
        peer = lax.rem(self.me + step, self.size)
        src = self.part.at[c, peer] if src is None else src
        return remote(
            self.name, peer, src, self.got.at[c, step - 1],
            self.send.at[c, step - 1], self.recv.at[c, step - 1],
        )

    def ends(self):
        last = self.size - 1
        return ((0, last, last, 1, last - 1), (last, 0, 1, last - 1, 2))

    def clear(self):
        if not self.relays:
            return
        for end, _, step, _, _ in self.ends():
            slot = self.size - step - 1

            @pl.when(self.me == end)
            def _():
                self.got[:, slot] = jnp.zeros(self.got.shape[:1] + self.got.shape[2:], self.got.dtype)

    def relay_copy(self, c, block, step, neighbour):
        return remote(
            self.name, neighbour, self.part.at[c, block], self.relay_in.at[c],
            self.send.at[c, step - 1], self.relay_recv.at[c],
        )

    def start(self, c):
        if self.relays:
            for end, block, step, neighbour, _ in self.ends():
                pl.when(self.me == end)(self.relay_copy(c, block, step, neighbour).start)
        for step in order(self.size):
            skips = []
            if self.relays:
                for end, _, far, neighbour, last in self.ends():
                    if step == far:
                        skips.append(self.me == end)
                    if step == last:
                        skips.append(self.me == neighbour)
            unless(skips, self.copy(c, step).start)

    def relay(self, c):
        if not self.relays:
            return
        for end, block, step, neighbour, last in self.ends():

            @pl.when(self.me == neighbour)
            def _():
                self.relay_copy(c, block, step, neighbour).wait_recv()
                total = self.relay_in[c].astype(F32) + self.part[c, block].astype(F32)
                self.relay_out[c] = total.astype(self.relay_out.dtype)
                self.copy(c, last, self.relay_out.at[c]).start()

    def total(self, c):
        for step in order(self.size):
            skips = []
            if self.relays:
                for end, _, far, _, _ in self.ends():
                    if step == self.size - far:
                        skips.append(self.me == end)
            unless(skips, self.copy(c, step).wait_recv)
        total = self.part[c, self.me].astype(F32)
        for slot in range(self.size - 1):
            total = total + self.got[c, slot].astype(F32)
        return total

    def finish(self, chunks):
        for c in range(chunks):
            for step in range(1, self.size):
                self.copy(c, step).wait_send()


class LineGather:
    def __init__(self, name, size, mine, everyone, send, recv, relay_send):
        self.name, self.size, self.me = name, size, lax.axis_index(name)
        self.mine, self.everyone = mine, everyone
        self.send, self.recv, self.relay_send = send, recv, relay_send
        self.relays = size >= 3

    def copy(self, c, step):
        peer = lax.rem(self.me + step, self.size)
        return remote(
            self.name, peer, self.mine.at[c], self.everyone.at[c, self.me],
            self.send.at[c, step - 1], self.recv.at[c, step - 1],
        )

    def skips(self, step):
        if not self.relays:
            return []
        skips = []
        if step != self.size - 1:
            skips.append(self.me == self.size - step)
        if step != 1:
            skips.append(self.me == self.size - 1 - step)
        return skips

    def start(self, c):
        for step in order(self.size):
            unless(self.skips(step), self.copy(c, step).start)

    def forwards(self):
        last = self.size - 1
        return ((1, 0, range(2, self.size)), (last - 1, last, range(last - 2, -1, -1)))

    def onward(self, c, end, source):
        step = (end - source) % self.size
        block = self.everyone.at[c, source]
        return remote(
            self.name, end, block, block, self.relay_send.at[c, source], self.recv.at[c, step - 1]
        )

    def forward(self, c):
        if not self.relays:
            return
        for neighbour, end, sources in self.forwards():

            @pl.when(self.me == neighbour)
            def _():
                for source in sources:
                    step = (neighbour - source) % self.size
                    self.copy(c, step).wait_recv()
                    self.onward(c, end, source).start()

    def wait(self, c):
        for step in order(self.size):
            skips = []
            if self.relays:
                if step != 1:
                    skips.append(self.me == 1)
                if step != self.size - 1:
                    skips.append(self.me == self.size - 2)
            unless(skips, self.copy(c, step).wait_recv)

    def finish(self, chunks):
        for c in range(chunks):
            for step in range(1, self.size):
                unless(self.skips(step), self.copy(c, step).wait_send)
            if self.relays:
                for neighbour, end, sources in self.forwards():

                    @pl.when(self.me == neighbour)
                    def _():
                        for source in sources:
                            self.onward(c, end, source).wait_send()


def silu(values):
    return values * jax.nn.sigmoid(values)


def softplus(values):
    return jnp.maximum(values, 0.0) + jnp.log1p(jnp.exp(-jnp.abs(values)))


def row_blocks(name, columns):
    return pl.ds(pl.multiple_of(lax.axis_index(name) * columns, LANES), columns)


def layer_kernel(
    n_kv, n_tp, width, head, repeat, chunks, pieces,
    stream, lengths, gain, decay_log, time_bias, out_gain, mlp_gain,
    w_b, w_d, w_q, w_k, w_v, w_g, q_hist, k_hist, v_hist, conv_q, conv_k, conv_v,
    w_out, w_up, w_down, state,
    result, new_state,
    stream_v, len_v, gain_v, dlog_v, bias_v, ogain_v, mgain_v,
    wb_v, wd_v, wq_v, wk_v, wv_v, wg_v, hist_q, hist_k, hist_v, convq_v, convk_v, convv_v,
    wo_v, wu_v, wdn_v,
    gains, params, streams, part_e, got_e,
    part_p, got_p, relay_pi, relay_po,
    key_s, query_s, value_s, fade_s, strength_s, dots_s, readouts,
    mine, gathered, mix_part, mix_got, mixed, blocks, sq_part, sq_got,
    up_part, up_got, relay_ui, relay_uo, hidden, hiddens, down_part, down_got,
    load_sem, state_sem, s_send, s_recv, e_send, e_recv,
    p_send, p_recv, p_relay, g_send, g_recv, g_relay,
    m_send, m_recv, b_send, b_recv, q_send, q_recv,
    u_send, u_recv, u_relay, h_send, h_recv, h_relay, d_send, d_recv,
):
    kv = lax.axis_index("kv")
    tp = lax.axis_index("tp")
    rows, own_cols = stream_v.shape
    own = rows // n_kv
    block = wq_v.shape[0]
    heads_all = w_b.shape[0]
    heads_own = chunks * repeat
    span = repeat * head
    block_cols = row_blocks("kv", block)

    sources = (
        (stream, stream_v),
        (gain, gain_v),
        (w_b.at[:, block_cols], wb_v), (w_d.at[:, block_cols], wd_v),
        (w_q, wq_v), (w_k, wk_v), (w_v, wv_v), (w_g, wg_v),
        (lengths, len_v), (decay_log, dlog_v), (time_bias, bias_v),
        (out_gain, ogain_v), (mlp_gain, mgain_v),
        (q_hist, hist_q), (k_hist, hist_k), (v_hist, hist_v),
        (conv_q.at[:, row_blocks("tp", convq_v.shape[1])], convq_v),
        (conv_k.at[:, row_blocks("tp", convk_v.shape[1])], convk_v),
        (conv_v.at[:, row_blocks("tp", convv_v.shape[1])], convv_v),
        (w_out, wo_v), (w_up, wu_v), (w_down, wdn_v),
    )
    loads = [pltpu.make_async_copy(src, dst, load_sem.at[i]) for i, (src, dst) in enumerate(sources)]
    state_loads = [
        pltpu.make_async_copy(
            state.at[:, c * repeat : (c + 1) * repeat],
            new_state.at[:, c * repeat : (c + 1) * repeat],
            state_sem.at[c],
        )
        for c in range(chunks)
    ]
    start(loads[:19])
    start(state_loads)
    start(loads[19:])

    scatter_p = LineScatter("kv", n_kv, part_p, got_p, relay_pi, relay_po, p_send, p_recv, p_relay)
    gather_g = LineGather("kv", n_kv, mine, gathered, g_send, g_recv, g_relay)
    scatter_u = LineScatter("kv", n_kv, up_part, up_got, relay_ui, relay_uo, u_send, u_recv, u_relay)
    gather_h = LineGather("kv", n_kv, hidden, hiddens, h_send, h_recv, h_relay)
    scatter_p.clear()
    scatter_u.clear()

    greet((("kv", n_kv), ("tp", n_tp)))
    loads[0].wait()
    stream_copies = gather_copies("tp", n_tp, stream_v, streams, s_send, s_recv)
    start(stream_copies)
    streams[tp] = stream_v[...]
    loads[1].wait()

    def gain_row(values):
        gains[...] = values[...].astype(F32)
        lines = block // LANES
        return jnp.concatenate(
            [gains[pl.ds(kv * lines + j, 1), :] for j in range(lines)], axis=1
        )

    norm_row = gain_row(gain_v)
    wait_recv(stream_copies)

    wide = jnp.concatenate([streams[t] for t in range(n_tp)], axis=1).astype(F32)
    scaled = (wide * norm_row).astype(BF16)
    squares = jnp.sum(wide * wide, axis=1, keepdims=True)
    loads[2].wait()
    loads[3].wait()
    beta = lax.dot_general(scaled, wb_v[...], CONTRACT_LAST, preferred_element_type=F32)
    decay = lax.dot_general(scaled, wd_v[...], CONTRACT_LAST, preferred_element_type=F32)
    part_e[...] = jnp.concatenate(
        [beta, decay, jnp.broadcast_to(squares, (rows, LANES - 2 * heads_all))], axis=1
    ).reshape(n_kv, own, LANES)
    extra_copies = scatter_copies("kv", n_kv, part_e, got_e, e_send, e_recv)
    start(extra_copies)

    for copy in loads[4:8]:
        copy.wait()
    fields = ((wq_v, head, 0), (wk_v, head, head), (wv_v, span, 2 * head), (wg_v, span, 2 * head + span))
    for c in range(chunks):
        for weight, size, offset in fields:
            product = jnp.dot(
                scaled, weight[:, c * size : (c + 1) * size], preferred_element_type=F32
            )
            part_p[c, :, :, offset : offset + size] = product.reshape(n_kv, own, size).astype(BF16)
        scatter_p.start(c)

    for copy in loads[8:19]:
        copy.wait()
    lens_row = jnp.broadcast_to(len_v[...].astype(F32), (own, own))
    diagonal = lax.broadcasted_iota(jnp.int32, (own, own), 0) == lax.broadcasted_iota(
        jnp.int32, (own, own), 1
    )
    length = jnp.sum(jnp.where(diagonal, lens_row, 0.0), axis=1, keepdims=True)

    def history(hist, taps):
        total = None
        count = taps.shape[0]
        for r in range(count - 1):
            live = length >= float(count - r)
            term = jnp.where(live, hist[r].astype(F32) * taps[r : r + 1, :], 0.0)
            total = term if total is None else total + term
        return total

    taps_q = convq_v[...].astype(F32)
    taps_k = convk_v[...].astype(F32)
    taps_v = convv_v[...].astype(F32)
    past_q = history(hist_q, taps_q)
    past_k = history(hist_k, taps_k)
    past_v = history(hist_v, taps_v)
    final = taps_q.shape[0] - 1

    params[...] = jnp.zeros(params.shape, F32)
    params[0:1, :heads_all] = dlog_v[...]
    params[1:2, :heads_all] = bias_v[...]
    shift = tp * heads_own
    own_params = pltpu.roll(params[...], lax.rem(LANES - shift, LANES), 1)

    wait_recv(extra_copies)
    extra = part_e[kv]
    for slot in range(n_kv - 1):
        extra = extra + got_e[slot]
    row_scale = lax.rsqrt(extra[:, 2 * heads_all : 2 * heads_all + 1] / width + EPSILON)
    terms = extra * row_scale
    own_beta = pltpu.roll(terms, lax.rem(LANES - shift, LANES), 1)
    own_decay = pltpu.roll(terms, lax.rem(2 * LANES - heads_all - shift, LANES), 1)
    fade = jnp.exp(-jnp.exp(own_params[0:1, :]) * softplus(own_decay + own_params[1:2, :]))
    fade = jnp.where(length == 1.0, 0.0, fade)
    strength = jax.nn.sigmoid(own_beta)
    gain_out = ogain_v[...].astype(F32)

    def unit(values, factor):
        return values * (
            lax.rsqrt(jnp.sum(values * values, axis=1, keepdims=True) + EPSILON) * factor
        )

    seqs = readouts.shape[1]

    def heads(c):
        total = scatter_p.total(c) * row_scale
        narrow = slice(c * head, (c + 1) * head)
        broad = slice(c * span, (c + 1) * span)
        query = unit(
            silu(total[:, :head] * taps_q[final : final + 1, narrow] + past_q[:, narrow]),
            head ** (-0.5),
        )
        key = unit(
            silu(total[:, head : 2 * head] * taps_k[final : final + 1, narrow] + past_k[:, narrow]),
            1.0,
        )
        query_s[...] = query
        key_s[...] = key
        value_s[...] = silu(
            total[:, 2 * head : 2 * head + span] * taps_v[final : final + 1, broad] + past_v[:, broad]
        )
        gate = silu(total[:, 2 * head + span :])
        dots_s[...] = jnp.broadcast_to(jnp.sum(query * key, axis=1, keepdims=True), (own, head))
        for j in range(repeat):
            v = c * repeat + j
            cols = slice(j * head, (j + 1) * head)
            fade_s[:, cols] = jnp.broadcast_to(fade[:, v : v + 1], (own, head))
            strength_s[:, cols] = jnp.broadcast_to(strength[:, v : v + 1], (own, head))
        state_loads[c].wait()

        @pl.loop(0, own // seqs)
        def _(g):
            base = g * seqs
            some = pl.ds(pl.multiple_of(base, seqs), seqs)
            keys_t = key_s[some, :].T
            queries_t = query_s[some, :].T
            dots = dots_s[some, :]
            values = value_s[some, :]
            fades = fade_s[some, :]
            strengths = strength_s[some, :]
            for s in range(seqs):
                key = jnp.broadcast_to(keys_t[:, s : s + 1], (head, head))
                query = jnp.broadcast_to(queries_t[:, s : s + 1], (head, head))
                line = slice(s, s + 1)
                for j in range(repeat):
                    cols = slice(j * head, (j + 1) * head)
                    held = new_state[base + s, c * repeat + j]
                    faded = fades[line, cols]
                    recalled = jnp.sum(held * key, axis=0, keepdims=True)
                    asked = jnp.sum(held * query, axis=0, keepdims=True)
                    update = strengths[line, cols] * (values[line, cols] - faded * recalled)
                    new_state[base + s, c * repeat + j] = held * faded + key * update
                    readouts[g, line, cols] = faded * asked + dots[line, :] * update

        for j in range(repeat):
            cols = slice(j * head, (j + 1) * head)
            one = readouts[:, :, cols].reshape(own, head)
            normed = one * lax.rsqrt(jnp.mean(one * one, axis=1, keepdims=True) + EPSILON)
            mine[c, :, cols] = (normed * gain_out * gate[:, cols]).astype(BF16)
        gather_g.start(c)
        gathered[c, kv] = mine[c]

    scatter_p.relay(0)
    for c in range(chunks):
        if c + 1 < chunks:
            scatter_p.relay(c + 1)
        heads(c)
        if c >= 1:
            gather_g.forward(c - 1)
    gather_g.forward(chunks - 1)

    def reduce_tp(product, part, got, send_sem, recv_sem):
        for t in range(n_tp):
            part[t] = product[:, t * own_cols : (t + 1) * own_cols].astype(BF16)
        copies = scatter_copies("tp", n_tp, part, got, send_sem, recv_sem)
        start(copies)
        wait_recv(copies)
        total = part[tp].astype(F32)
        for slot in range(n_tp - 1):
            total = total + got[slot].astype(F32)
        return total, copies

    loads[19].wait()
    product = jnp.zeros((rows, wo_v.shape[1]), F32)
    for c in range(chunks):
        gather_g.wait(c)
        product = product + jnp.dot(
            gathered[c].reshape(rows, span),
            wo_v[c * span : (c + 1) * span, :],
            preferred_element_type=F32,
        )
    total, mix_copies = reduce_tp(product, mix_part, mix_got, m_send, m_recv)
    mixed_own = (stream_v[...].astype(F32) + total).astype(BF16)
    mixed[...] = mixed_own
    block_copies = gather_copies("tp", n_tp, mixed, blocks, b_send, b_recv)
    start(block_copies)
    blocks[tp] = mixed_own
    mlp_row = gain_row(mgain_v)
    loads[20].wait()
    wait_recv(block_copies)
    wide = jnp.concatenate([blocks[t] for t in range(n_tp)], axis=1).astype(F32)
    scaled = (wide * mlp_row).astype(BF16)
    squares = jnp.sum(wide * wide, axis=1, keepdims=True)
    sq_part[...] = jnp.broadcast_to(squares, (rows, LANES)).reshape(n_kv, own, LANES)
    square_copies = scatter_copies("kv", n_kv, sq_part, sq_got, q_send, q_recv)
    start(square_copies)
    piece = wu_v.shape[1] // pieces
    for p in range(pieces):
        product = jnp.dot(
            scaled, wu_v[:, p * piece : (p + 1) * piece], preferred_element_type=F32
        )
        up_part[p] = product.reshape(n_kv, own, piece).astype(BF16)
        scatter_u.start(p)
    wait_recv(square_copies)
    square_sum = sq_part[kv]
    for slot in range(n_kv - 1):
        square_sum = square_sum + sq_got[slot]
    unit_scale = lax.rsqrt(square_sum[:, :1] / width + EPSILON)

    def activate(p):
        active = jnp.maximum(scatter_u.total(p) * unit_scale, 0.0)
        active = (active * active).astype(BF16)
        hidden[p] = active
        gather_h.start(p)
        hiddens[p, kv] = active

    scatter_u.relay(0)
    for p in range(pieces):
        if p + 1 < pieces:
            scatter_u.relay(p + 1)
        activate(p)
        if p >= 1:
            gather_h.forward(p - 1)
    gather_h.forward(pieces - 1)
    loads[21].wait()
    product = jnp.zeros((rows, wdn_v.shape[1]), F32)
    for p in range(pieces):
        gather_h.wait(p)
        product = product + jnp.dot(
            hiddens[p].reshape(rows, piece),
            wdn_v[p * piece : (p + 1) * piece, :],
            preferred_element_type=F32,
        )
    total, down_copies = reduce_tp(product, down_part, down_got, d_send, d_recv)
    result[...] = (mixed[...].astype(F32) + total).astype(BF16)
    for copies in (stream_copies, extra_copies, mix_copies, block_copies, square_copies, down_copies):
        wait_send(copies)
    scatter_p.finish(chunks)
    gather_g.finish(chunks)
    scatter_u.finish(pieces)
    gather_h.finish(pieces)


def on_device(
    n_kv, n_tp,
    stream, lengths, delta_state, q_hist, k_hist, v_hist, norm_gain,
    w_query, w_key, w_value, w_gate, w_beta, w_decay,
    conv_query, conv_key, conv_value, decay_log, time_bias, out_gain,
    w_out, mlp_gain, w_up, w_down,
):
    width = norm_gain.shape[0]
    rows, own_cols = stream.shape
    own, heads_own, head = delta_state.shape[:3]
    key_cols = q_hist.shape[2]
    value_cols = v_hist.shape[2]
    block = w_query.shape[0]
    heads_all = w_beta.shape[1]
    taps = conv_query.shape[0]
    chunks = key_cols // head
    repeat = heads_own // chunks
    span = repeat * head
    field = 2 * head + 2 * span
    units = w_up.shape[1]
    pieces = 4
    piece = units // pieces
    seqs = min(8, own)
    vmem = pl.BlockSpec(memory_space=pltpu.VMEM)
    hbm = pl.BlockSpec(memory_space=pltpu.HBM)
    dma = pltpu.SemaphoreType.DMA
    gain_shape = (width // LANES, LANES)
    ins = (
        stream, lengths[None], norm_gain.reshape(gain_shape), decay_log[None], time_bias[None],
        out_gain[None], mlp_gain.reshape(gain_shape),
        w_beta.T, w_decay.T, w_query, w_key, w_value, w_gate,
        *(jnp.transpose(hist, (1, 0, 2)) for hist in (q_hist, k_hist, v_hist)),
        conv_query, conv_key, conv_value, w_out, w_up, w_down, delta_state,
    )

    def buffer(*dims, dtype=BF16):
        return pltpu.VMEM(dims, dtype)

    result, new_state = pl.pallas_call(
        functools.partial(layer_kernel, n_kv, n_tp, width, head, repeat, chunks, pieces),
        out_shape=(
            pltpu.VMEM((rows, own_cols), BF16),
            pltpu.VMEM(delta_state.shape, F32),
        ),
        in_specs=[hbm] * len(ins),
        out_specs=(vmem, vmem),
        scratch_shapes=[
            buffer(rows, own_cols), buffer(1, own, dtype=jnp.int32), buffer(*gain_shape),
            buffer(1, heads_all, dtype=F32), buffer(1, heads_all, dtype=F32),
            buffer(1, head), buffer(*gain_shape),
            buffer(heads_all, block), buffer(heads_all, block),
            buffer(block, key_cols), buffer(block, key_cols),
            buffer(block, value_cols), buffer(block, value_cols),
            buffer(taps - 1, own, key_cols), buffer(taps - 1, own, key_cols),
            buffer(taps - 1, own, value_cols),
            buffer(taps, key_cols), buffer(taps, key_cols), buffer(taps, value_cols),
            buffer(*w_out.shape), buffer(*w_up.shape), buffer(*w_down.shape),
            buffer(*gain_shape, dtype=F32), buffer(8, LANES, dtype=F32),
            buffer(n_tp, rows, own_cols),
            buffer(n_kv, own, LANES, dtype=F32), buffer(n_kv - 1, own, LANES, dtype=F32),
            buffer(chunks, n_kv, own, field), buffer(chunks, n_kv - 1, own, field),
            buffer(chunks, own, field), buffer(chunks, own, field),
            buffer(own, head, dtype=F32), buffer(own, head, dtype=F32),
            buffer(own, span, dtype=F32), buffer(own, span, dtype=F32),
            buffer(own, span, dtype=F32), buffer(own, head, dtype=F32),
            buffer(own // seqs, seqs, span, dtype=F32),
            buffer(chunks, own, span), buffer(chunks, n_kv, own, span),
            buffer(n_tp, rows, own_cols), buffer(n_tp - 1, rows, own_cols),
            buffer(rows, own_cols), buffer(n_tp, rows, own_cols),
            buffer(n_kv, own, LANES, dtype=F32), buffer(n_kv - 1, own, LANES, dtype=F32),
            buffer(pieces, n_kv, own, piece), buffer(pieces, n_kv - 1, own, piece),
            buffer(pieces, own, piece), buffer(pieces, own, piece),
            buffer(pieces, own, piece), buffer(pieces, n_kv, own, piece),
            buffer(n_tp, rows, own_cols), buffer(n_tp - 1, rows, own_cols),
            dma((22,)), dma((chunks,)),
            dma((n_tp - 1,)), dma((n_tp - 1,)),
            dma((n_kv - 1,)), dma((n_kv - 1,)),
            dma((chunks, n_kv - 1)), dma((chunks, n_kv - 1)), dma((chunks,)),
            dma((chunks, n_kv - 1)), dma((chunks, n_kv - 1)), dma((chunks, n_kv)),
            dma((n_tp - 1,)), dma((n_tp - 1,)),
            dma((n_tp - 1,)), dma((n_tp - 1,)),
            dma((n_kv - 1,)), dma((n_kv - 1,)),
            dma((pieces, n_kv - 1)), dma((pieces, n_kv - 1)), dma((pieces,)),
            dma((pieces, n_kv - 1)), dma((pieces, n_kv - 1)), dma((pieces, n_kv)),
            dma((n_tp - 1,)), dma((n_tp - 1,)),
        ],
        compiler_params=pltpu.CompilerParams(
            collective_id=0, has_side_effects=True,
            vmem_limit_bytes=67043328 - delta_state.size * 4 - 2**18,
        ),
        name="layer",
    )(*ins)
    return result, new_state


def solution(mesh):
    in_specs = (
        P("grp", ("kv", "tp")),
        P(("grp", "kv")),
        P(("grp", "kv"), "tp", None, None),
        P(("grp", "kv"), None, "tp"),
        P(("grp", "kv"), None, "tp"),
        P(("grp", "kv"), None, "tp"),
        P(),
        P("kv", "tp"),
        P("kv", "tp"),
        P("kv", "tp"),
        P("kv", "tp"),
        P(),
        P(),
        P(),
        P(),
        P(),
        P(),
        P(),
        P(),
        P("tp", "kv"),
        P(),
        P("kv", "tp"),
        P("tp", "kv"),
    )
    out_specs = (P("grp", ("kv", "tp")), P(("grp", "kv"), "tp", None, None))
    return jax.shard_map(
        functools.partial(on_device, mesh.shape["kv"], mesh.shape["tp"]),
        mesh=mesh, in_specs=in_specs, out_specs=out_specs, check_vma=False,
    )
```

time: 104 us -> 80.5 us (0.77)
  Pallas kernels: 91.3 us -> 72.9 us
  local copies, waits for them, and re-layouts: 10 us -> 6.78 us
  other arithmetic: 1.27 us -> 0 us
    pallas_call x3 -> x1, Pallas kernels: 91.3 us -> 72.9 us  [on_device(): pl.pallas_call(functools.partial(layer_kernel, n_kv, n_tp, width, head, r...]
    broadcast_in_dim x3 -> x0, local copies, waits for them, and re-layouts: 3.31 us -> none  [the longest x1 1.33 us: on_device(): wide_lengths = jnp.broadcast_to(lengths[:, None], (own, LANES))]
    another operation x1 -> x0, other arithmetic: 1.27 us -> none  [on_device(): jnp.stack([decay_log, time_bias])]
    unnamed x11 -> x2, local copies, waits for them, and re-layouts: 6.68 us -> 6.78 us
where the time goes in v1:
time: 80.5 us; the launch traced here: 80.3 us
  Pallas kernels  72.9 us (91%)
  local copies, waits for them, and re-layouts  6.78 us (8%)
    pallas_call x1, Pallas kernels, on_device(): pl.pallas_call(functools.partial(layer_kernel, n_kv, n_tp, width, head, r...  72.9 us
    unnamed x2, local copies, waits for them, and re-layouts  6.78 us

profile of v1, /device:TPU:0, one launch (start us, length us, event | category | flops | bytes accessed | tf_op | source)
XLA Modules:
  0.0 80.3 jit_solution(7491367381412109305)
XLA Ops:
  0.6 72.9 %layer.1 = (bf16[128,128]{1,0:T(8,128)(2,1)S(1)}, f32[32,8,128,128]{3,2,1,0:T(8,128)S(1)}) custom-call(bf16[128,128]{1,0:T(8,128)(2,1)} %stream.1, s32[1,32]{1,0:T(1,128)} %bitcast.18, bf16[16,128]{1,0:T(8,128)(2,1)} %bitcast.16, f32[1,32]{1,0:T(1,128)} %bitcast.19, f32[1,32]{1,0:T(1,128)} %bitcast.20, bf16[1,128]{1,0:T(2,128)(2,1)} %bitcast.21, ...), custom_call_target="tpu_custom_call" | custom-call | tf_op jit(solution)/shard_map/layer/pallas_call | solution.py:595
  73.6 0.6 copy.27
  74.2 6.2 %copy.28 = f32[32,8,128,128]{3,2,1,0:T(8,128)} copy(f32[32,8,128,128]{3,2,1,0:T(8,128)S(1)} %get-tuple-element.3) | data formatting | bytes 33554432

commit v2 on v1

--- a/solution.py
+++ b/solution.py
@@ -12,6 +12,8 @@
 F32 = jnp.float32
 BF16 = jnp.bfloat16
 LANES = 128
+LEAD = 1
+DIRECT_LAST = 1
 CONTRACT_LAST = (((1,), (1,)), ((), ()))
 
 
@@ -90,6 +92,7 @@
         self.part, self.got = part, got
         self.relay_in, self.relay_out = relay_in, relay_out
         self.send, self.recv, self.relay_recv = send, recv, relay_recv
+        self.chunks = part.shape[0]
         self.relays = size >= 4
 
     def copy(self, c, step, src=None):
@@ -130,7 +133,7 @@
                 for end, _, far, neighbour, last in self.ends():
                     if step == far:
                         skips.append(self.me == end)
-                    if step == last:
+                    if step == last or c >= LEAD:
                         skips.append(self.me == neighbour)
             unless(skips, self.copy(c, step).start)
 
@@ -145,6 +148,10 @@
                 total = self.relay_in[c].astype(F32) + self.part[c, block].astype(F32)
                 self.relay_out[c] = total.astype(self.relay_out.dtype)
                 self.copy(c, last, self.relay_out.at[c]).start()
+                if c + LEAD < self.chunks:
+                    for hop in order(self.size):
+                        if hop != last:
+                            self.copy(c + LEAD, hop).start()
 
     def total(self, c):
         for step in order(self.size):
@@ -171,6 +178,7 @@
         self.mine, self.everyone = mine, everyone
         self.send, self.recv, self.relay_send = send, recv, relay_send
         self.relays = size >= 3
+        self.direct = () if DIRECT_LAST == 0 else range(mine.shape[0] - DIRECT_LAST, mine.shape[0])
 
     def copy(self, c, step):
         peer = lax.rem(self.me + step, self.size)
@@ -179,8 +187,8 @@
             self.send.at[c, step - 1], self.recv.at[c, step - 1],
         )
 
-    def skips(self, step):
-        if not self.relays:
+    def skips(self, c, step):
+        if not self.relays or c in self.direct:
             return []
         skips = []
         if step != self.size - 1:
@@ -191,7 +199,7 @@
 
     def start(self, c):
         for step in order(self.size):
-            unless(self.skips(step), self.copy(c, step).start)
+            unless(self.skips(c, step), self.copy(c, step).start)
 
     def forwards(self):
         last = self.size - 1
@@ -205,7 +213,7 @@
         )
 
     def forward(self, c):
-        if not self.relays:
+        if not self.relays or c in self.direct:
             return
         for neighbour, end, sources in self.forwards():
 
@@ -219,7 +227,7 @@
     def wait(self, c):
         for step in order(self.size):
             skips = []
-            if self.relays:
+            if self.relays and c not in self.direct:
                 if step != 1:
                     skips.append(self.me == 1)
                 if step != self.size - 1:
@@ -229,8 +237,8 @@
     def finish(self, chunks):
         for c in range(chunks):
             for step in range(1, self.size):
-                unless(self.skips(step), self.copy(c, step).wait_send)
-            if self.relays:
+                unless(self.skips(c, step), self.copy(c, step).wait_send)
+            if self.relays and c not in self.direct:
                 for neighbour, end, sources in self.forwards():
 
                     @pl.when(self.me == neighbour)
@@ -262,7 +270,7 @@
     wo_v, wu_v, wdn_v,
     gains, params, streams, part_e, got_e,
     part_p, got_p, relay_pi, relay_po,
-    key_s, query_s, value_s, fade_s, strength_s, dots_s, readouts,
+    readouts,
     mine, gathered, mix_part, mix_got, mixed, blocks, sq_part, sq_got,
     up_part, up_got, relay_ui, relay_uo, hidden, hiddens, down_part, down_got,
     load_sem, state_sem, s_send, s_recv, e_send, e_recv,
@@ -417,43 +425,56 @@
             silu(total[:, head : 2 * head] * taps_k[final : final + 1, narrow] + past_k[:, narrow]),
             1.0,
         )
-        query_s[...] = query
-        key_s[...] = key
-        value_s[...] = silu(
+        values = silu(
             total[:, 2 * head : 2 * head + span] * taps_v[final : final + 1, broad] + past_v[:, broad]
         )
         gate = silu(total[:, 2 * head + span :])
-        dots_s[...] = jnp.broadcast_to(jnp.sum(query * key, axis=1, keepdims=True), (own, head))
-        for j in range(repeat):
-            v = c * repeat + j
-            cols = slice(j * head, (j + 1) * head)
-            fade_s[:, cols] = jnp.broadcast_to(fade[:, v : v + 1], (own, head))
-            strength_s[:, cols] = jnp.broadcast_to(strength[:, v : v + 1], (own, head))
+        dot = jnp.sum(query * key, axis=1, keepdims=True)
+        owned = range(c * repeat, (c + 1) * repeat)
+
+        def widen(columns):
+            return jnp.concatenate(
+                [jnp.broadcast_to(column, (own, head)) for column in columns], axis=1
+            )
+
+        dots = widen([dot] * repeat)
+        fades = widen([fade[:, v : v + 1] for v in owned])
+        strengths = widen([strength[:, v : v + 1] for v in owned])
+        keys_t = key.T
+        line = lax.broadcasted_iota(jnp.int32, (seqs, span), 0)
         state_loads[c].wait()
 
-        @pl.loop(0, own // seqs)
-        def _(g):
-            base = g * seqs
-            some = pl.ds(pl.multiple_of(base, seqs), seqs)
-            keys_t = key_s[some, :].T
-            queries_t = query_s[some, :].T
-            dots = dots_s[some, :]
-            values = value_s[some, :]
-            fades = fade_s[some, :]
-            strengths = strength_s[some, :]
+        def ask(g):
+            some = slice(g * seqs, (g + 1) * seqs)
+            both = jnp.concatenate([key[some], query[some]], axis=0).astype(BF16)
+            recalled = jnp.zeros((seqs, span), F32)
+            asked = jnp.zeros((seqs, span), F32)
             for s in range(seqs):
-                key = jnp.broadcast_to(keys_t[:, s : s + 1], (head, head))
-                query = jnp.broadcast_to(queries_t[:, s : s + 1], (head, head))
-                line = slice(s, s + 1)
-                for j in range(repeat):
+                held = jnp.concatenate([new_state[g * seqs + s, v] for v in owned], axis=1)
+                answer = jnp.dot(both, held.astype(BF16), preferred_element_type=F32)
+                recalled = jnp.where(line == s, answer[:seqs], recalled)
+                asked = jnp.where(line == s, answer[seqs:], asked)
+            faded = fades[some]
+            update = strengths[some] * (values[some] - faded * recalled)
+            readouts[g] = faded * asked + dots[some] * update
+            return faded, update
+
+        def apply(g, faded, update):
+            for s in range(seqs):
+                q = g * seqs + s
+                wide_key = jnp.broadcast_to(keys_t[:, q : q + 1], (head, head))
+                for j, v in enumerate(owned):
                     cols = slice(j * head, (j + 1) * head)
-                    held = new_state[base + s, c * repeat + j]
-                    faded = fades[line, cols]
-                    recalled = jnp.sum(held * key, axis=0, keepdims=True)
-                    asked = jnp.sum(held * query, axis=0, keepdims=True)
-                    update = strengths[line, cols] * (values[line, cols] - faded * recalled)
-                    new_state[base + s, c * repeat + j] = held * faded + key * update
-                    readouts[g, line, cols] = faded * asked + dots[line, :] * update
+                    new_state[q, v] = (
+                        new_state[q, v] * faded[s : s + 1, cols] + wide_key * update[s : s + 1, cols]
+                    )
+
+        groups = own // seqs
+        ready = ask(0)
+        for g in range(groups):
+            later = ask(g + 1) if g + 1 < groups else None
+            apply(g, *ready)
+            ready = later
 
         for j in range(repeat):
             cols = slice(j * head, (j + 1) * head)
@@ -468,15 +489,18 @@
         if c + 1 < chunks:
             scatter_p.relay(c + 1)
         heads(c)
-        if c >= 1:
-            gather_g.forward(c - 1)
-    gather_g.forward(chunks - 1)
-
-    def reduce_tp(product, part, got, send_sem, recv_sem):
+        if c == chunks - 2:
+            gather_g.forward(0)
+    for c in range(1 if chunks > 1 else 0, chunks):
+        gather_g.forward(c)
+
+    def reduce_tp(product, part, got, send_sem, recv_sem, meanwhile=None):
         for t in range(n_tp):
             part[t] = product[:, t * own_cols : (t + 1) * own_cols].astype(BF16)
         copies = scatter_copies("tp", n_tp, part, got, send_sem, recv_sem)
         start(copies)
+        if meanwhile is not None:
+            meanwhile()
         wait_recv(copies)
         total = part[tp].astype(F32)
         for slot in range(n_tp - 1):
@@ -503,10 +527,6 @@
     wait_recv(block_copies)
     wide = jnp.concatenate([blocks[t] for t in range(n_tp)], axis=1).astype(F32)
     scaled = (wide * mlp_row).astype(BF16)
-    squares = jnp.sum(wide * wide, axis=1, keepdims=True)
-    sq_part[...] = jnp.broadcast_to(squares, (rows, LANES)).reshape(n_kv, own, LANES)
-    square_copies = scatter_copies("kv", n_kv, sq_part, sq_got, q_send, q_recv)
-    start(square_copies)
     piece = wu_v.shape[1] // pieces
     for p in range(pieces):
         product = jnp.dot(
@@ -514,14 +534,20 @@
         )
         up_part[p] = product.reshape(n_kv, own, piece).astype(BF16)
         scatter_u.start(p)
-    wait_recv(square_copies)
-    square_sum = sq_part[kv]
-    for slot in range(n_kv - 1):
-        square_sum = square_sum + sq_got[slot]
-    unit_scale = lax.rsqrt(square_sum[:, :1] / width + EPSILON)
+    corner = lax.broadcasted_iota(jnp.int32, (rows, rows), 0) == lax.broadcasted_iota(
+        jnp.int32, (rows, rows), 1
+    )
+    squares = jnp.sum(wide * wide, axis=1, keepdims=True)
+    flat = jnp.sum(jnp.where(corner, squares, 0.0), axis=0, keepdims=True)
+    sq_part[...] = jnp.broadcast_to(flat, sq_part.shape)
+    square_copies = gather_copies("kv", n_kv, sq_part, sq_got, q_send, q_recv)
+    start(square_copies)
+    sq_got[kv] = sq_part[...]
+    scatter_p.finish(chunks)
+    gather_g.finish(chunks)
 
     def activate(p):
-        active = jnp.maximum(scatter_u.total(p) * unit_scale, 0.0)
+        active = jnp.maximum(scatter_u.total(p), 0.0)
         active = (active * active).astype(BF16)
         hidden[p] = active
         gather_h.start(p)
@@ -532,10 +558,15 @@
         if p + 1 < pieces:
             scatter_u.relay(p + 1)
         activate(p)
-        if p >= 1:
-            gather_h.forward(p - 1)
-    gather_h.forward(pieces - 1)
+    for p in range(pieces):
+        gather_h.forward(p)
     loads[21].wait()
+    wait_recv(square_copies)
+    square_sum = sq_got[0]
+    for z in range(1, n_kv):
+        square_sum = square_sum + sq_got[z]
+    spread = jnp.broadcast_to(1.0 / (square_sum[0:1, :] / width + EPSILON), (rows, rows))
+    scale_squared = jnp.sum(jnp.where(corner, spread, 0.0), axis=1, keepdims=True)
     product = jnp.zeros((rows, wdn_v.shape[1]), F32)
     for p in range(pieces):
         gather_h.wait(p)
@@ -544,14 +575,18 @@
             wdn_v[p * piece : (p + 1) * piece, :],
             preferred_element_type=F32,
         )
-    total, down_copies = reduce_tp(product, down_part, down_got, d_send, d_recv)
+
+    def settle():
+        for copies in (stream_copies, extra_copies, mix_copies, block_copies, square_copies):
+            wait_send(copies)
+        scatter_u.finish(pieces)
+        gather_h.finish(pieces)
+
+    total, down_copies = reduce_tp(
+        product * scale_squared, down_part, down_got, d_send, d_recv, settle
+    )
     result[...] = (mixed[...].astype(F32) + total).astype(BF16)
-    for copies in (stream_copies, extra_copies, mix_copies, block_copies, square_copies, down_copies):
-        wait_send(copies)
-    scatter_p.finish(chunks)
-    gather_g.finish(chunks)
-    scatter_u.finish(pieces)
-    gather_h.finish(pieces)
+    wait_send(down_copies)
 
 
 def on_device(
@@ -616,14 +651,11 @@
             buffer(n_kv, own, LANES, dtype=F32), buffer(n_kv - 1, own, LANES, dtype=F32),
             buffer(chunks, n_kv, own, field), buffer(chunks, n_kv - 1, own, field),
             buffer(chunks, own, field), buffer(chunks, own, field),
-            buffer(own, head, dtype=F32), buffer(own, head, dtype=F32),
-            buffer(own, span, dtype=F32), buffer(own, span, dtype=F32),
-            buffer(own, span, dtype=F32), buffer(own, head, dtype=F32),
             buffer(own // seqs, seqs, span, dtype=F32),
             buffer(chunks, own, span), buffer(chunks, n_kv, own, span),
             buffer(n_tp, rows, own_cols), buffer(n_tp - 1, rows, own_cols),
             buffer(rows, own_cols), buffer(n_tp, rows, own_cols),
-            buffer(n_kv, own, LANES, dtype=F32), buffer(n_kv - 1, own, LANES, dtype=F32),
+            buffer(8, rows, dtype=F32), buffer(n_kv, 8, rows, dtype=F32),
             buffer(pieces, n_kv, own, piece), buffer(pieces, n_kv - 1, own, piece),
             buffer(pieces, own, piece), buffer(pieces, own, piece),
             buffer(pieces, own, piece), buffer(pieces, n_kv, own, piece),

time: 80.5 us -> 72.7 us (0.903)
  Pallas kernels: 72.9 us -> 65.2 us
    pallas_call x1, Pallas kernels: 72.9 us -> 65.2 us  [on_device(): pl.pallas_call(functools.partial(layer_kernel, n_kv, n_tp, width, head, r...]
where the time goes in v2:
time: 72.7 us; the launch traced here: 72.6 us
  Pallas kernels  65.2 us (90%)
  local copies, waits for them, and re-layouts  6.78 us (9%)
    pallas_call x1, Pallas kernels, on_device(): pl.pallas_call(functools.partial(layer_kernel, n_kv, n_tp, width, head, r...  65.2 us
    unnamed x2, local copies, waits for them, and re-layouts  6.78 us

profile of v2, /device:TPU:0, one launch (start us, length us, event | category | flops | bytes accessed | tf_op | source)
XLA Modules:
  0.0 72.6 jit_solution(9626251814673288860)
XLA Ops:
  0.6 65.2 %layer.1 = (bf16[128,128]{1,0:T(8,128)(2,1)S(1)}, f32[32,8,128,128]{3,2,1,0:T(8,128)S(1)}) custom-call(bf16[128,128]{1,0:T(8,128)(2,1)} %stream.1, s32[1,32]{1,0:T(1,128)} %bitcast.18, bf16[16,128]{1,0:T(8,128)(2,1)} %bitcast.16, f32[1,32]{1,0:T(1,128)} %bitcast.19, f32[1,32]{1,0:T(1,128)} %bitcast.20, bf16[1,128]{1,0:T(2,128)(2,1)} %bitcast.21, ...), custom_call_target="tpu_custom_call" | custom-call | tf_op jit(solution)/shard_map/layer/pallas_call | solution.py:630
  65.8 0.6 copy.27
  66.4 6.2 %copy.28 = f32[32,8,128,128]{3,2,1,0:T(8,128)} copy(f32[32,8,128,128]{3,2,1,0:T(8,128)S(1)} %get-tuple-element.3) | data formatting | bytes 33554432

commit v3 on v2

--- a/solution.py
+++ b/solution.py
@@ -12,7 +12,7 @@
 F32 = jnp.float32
 BF16 = jnp.bfloat16
 LANES = 128
-LEAD = 1
+LEAD = 2
 DIRECT_LAST = 1
 CONTRACT_LAST = (((1,), (1,)), ((), ()))
 
@@ -87,12 +87,14 @@
 
 
 class LineScatter:
-    def __init__(self, name, size, part, got, relay_in, relay_out, send, recv, relay_recv):
+    def __init__(
+        self, name, size, group, part, got, relay_in, relay_out, send, recv, relay_recv
+    ):
         self.name, self.size, self.me = name, size, lax.axis_index(name)
         self.part, self.got = part, got
         self.relay_in, self.relay_out = relay_in, relay_out
         self.send, self.recv, self.relay_recv = send, recv, relay_recv
-        self.chunks = part.shape[0]
+        self.chunks, self.group = part.shape[0], group
         self.relays = size >= 4
 
     def copy(self, c, step, src=None):
@@ -133,7 +135,7 @@
                 for end, _, far, neighbour, last in self.ends():
                     if step == far:
                         skips.append(self.me == end)
-                    if step == last or c >= LEAD:
+                    if step == last or c % self.group >= LEAD:
                         skips.append(self.me == neighbour)
             unless(skips, self.copy(c, step).start)
 
@@ -148,7 +150,7 @@
                 total = self.relay_in[c].astype(F32) + self.part[c, block].astype(F32)
                 self.relay_out[c] = total.astype(self.relay_out.dtype)
                 self.copy(c, last, self.relay_out.at[c]).start()
-                if c + LEAD < self.chunks:
+                if c + LEAD < self.chunks and (c + LEAD) % self.group >= LEAD:
                     for hop in order(self.size):
                         if hop != last:
                             self.copy(c + LEAD, hop).start()
@@ -173,12 +175,12 @@
 
 
 class LineGather:
-    def __init__(self, name, size, mine, everyone, send, recv, relay_send):
+    def __init__(self, name, size, group, mine, everyone, send, recv, relay_send):
         self.name, self.size, self.me = name, size, lax.axis_index(name)
         self.mine, self.everyone = mine, everyone
         self.send, self.recv, self.relay_send = send, recv, relay_send
         self.relays = size >= 3
-        self.direct = () if DIRECT_LAST == 0 else range(mine.shape[0] - DIRECT_LAST, mine.shape[0])
+        self.direct = [c for c in range(mine.shape[0]) if c % group >= group - DIRECT_LAST]
 
     def copy(self, c, step):
         peer = lax.rem(self.me + step, self.size)
@@ -260,7 +262,7 @@
 
 
 def layer_kernel(
-    n_kv, n_tp, width, head, repeat, chunks, pieces,
+    n_kv, n_tp, width, head, repeat, chunks, pieces, halves,
     stream, lengths, gain, decay_log, time_bias, out_gain, mlp_gain,
     w_b, w_d, w_q, w_k, w_v, w_g, q_hist, k_hist, v_hist, conv_q, conv_k, conv_v,
     w_out, w_up, w_down, state,
@@ -282,6 +284,8 @@
     tp = lax.axis_index("tp")
     rows, own_cols = stream_v.shape
     own = rows // n_kv
+    share = own // halves
+    half_rows = n_kv * share
     block = wq_v.shape[0]
     heads_all = w_b.shape[0]
     heads_own = chunks * repeat
@@ -314,10 +318,10 @@
     start(state_loads)
     start(loads[19:])
 
-    scatter_p = LineScatter("kv", n_kv, part_p, got_p, relay_pi, relay_po, p_send, p_recv, p_relay)
-    gather_g = LineGather("kv", n_kv, mine, gathered, g_send, g_recv, g_relay)
-    scatter_u = LineScatter("kv", n_kv, up_part, up_got, relay_ui, relay_uo, u_send, u_recv, u_relay)
-    gather_h = LineGather("kv", n_kv, hidden, hiddens, h_send, h_recv, h_relay)
+    scatter_p = LineScatter("kv", n_kv, halves * chunks, part_p, got_p, relay_pi, relay_po, p_send, p_recv, p_relay)
+    gather_g = LineGather("kv", n_kv, chunks, mine, gathered, g_send, g_recv, g_relay)
+    scatter_u = LineScatter("kv", n_kv, pieces, up_part, up_got, relay_ui, relay_uo, u_send, u_recv, u_relay)
+    gather_h = LineGather("kv", n_kv, pieces, hidden, hiddens, h_send, h_recv, h_relay)
     scatter_p.clear()
     scatter_u.clear()
 
@@ -359,7 +363,11 @@
             product = jnp.dot(
                 scaled, weight[:, c * size : (c + 1) * size], preferred_element_type=F32
             )
-            part_p[c, :, :, offset : offset + size] = product.reshape(n_kv, own, size).astype(BF16)
+            split = product.reshape(n_kv, own, size).astype(BF16)
+            for h in range(halves):
+                part_p[h * chunks + c, :, :, offset : offset + size] = split[
+                    :, h * share : (h + 1) * share
+                ]
         scatter_p.start(c)
 
     for copy in loads[8:19]:
@@ -413,20 +421,22 @@
 
     seqs = readouts.shape[1]
 
-    def heads(c):
-        total = scatter_p.total(c) * row_scale
+    def heads(h, c):
+        index = h * chunks + c
+        these = slice(h * share, (h + 1) * share)
+        total = scatter_p.total(index) * row_scale[these]
         narrow = slice(c * head, (c + 1) * head)
         broad = slice(c * span, (c + 1) * span)
         query = unit(
-            silu(total[:, :head] * taps_q[final : final + 1, narrow] + past_q[:, narrow]),
+            silu(total[:, :head] * taps_q[final : final + 1, narrow] + past_q[these, narrow]),
             head ** (-0.5),
         )
         key = unit(
-            silu(total[:, head : 2 * head] * taps_k[final : final + 1, narrow] + past_k[:, narrow]),
+            silu(total[:, head : 2 * head] * taps_k[final : final + 1, narrow] + past_k[these, narrow]),
             1.0,
         )
         values = silu(
-            total[:, 2 * head : 2 * head + span] * taps_v[final : final + 1, broad] + past_v[:, broad]
+            total[:, 2 * head : 2 * head + span] * taps_v[final : final + 1, broad] + past_v[these, broad]
         )
         gate = silu(total[:, 2 * head + span :])
         dot = jnp.sum(query * key, axis=1, keepdims=True)
@@ -434,15 +444,16 @@
 
         def widen(columns):
             return jnp.concatenate(
-                [jnp.broadcast_to(column, (own, head)) for column in columns], axis=1
+                [jnp.broadcast_to(column, (share, head)) for column in columns], axis=1
             )
 
         dots = widen([dot] * repeat)
-        fades = widen([fade[:, v : v + 1] for v in owned])
-        strengths = widen([strength[:, v : v + 1] for v in owned])
+        fades = widen([fade[these, v : v + 1] for v in owned])
+        strengths = widen([strength[these, v : v + 1] for v in owned])
         keys_t = key.T
         line = lax.broadcasted_iota(jnp.int32, (seqs, span), 0)
-        state_loads[c].wait()
+        if h == 0:
+            state_loads[c].wait()
 
         def ask(g):
             some = slice(g * seqs, (g + 1) * seqs)
@@ -450,7 +461,8 @@
             recalled = jnp.zeros((seqs, span), F32)
             asked = jnp.zeros((seqs, span), F32)
             for s in range(seqs):
-                held = jnp.concatenate([new_state[g * seqs + s, v] for v in owned], axis=1)
+                q = h * share + g * seqs + s
+                held = jnp.concatenate([new_state[q, v] for v in owned], axis=1)
                 answer = jnp.dot(both, held.astype(BF16), preferred_element_type=F32)
                 recalled = jnp.where(line == s, answer[:seqs], recalled)
                 asked = jnp.where(line == s, answer[seqs:], asked)
@@ -461,15 +473,16 @@
 
         def apply(g, faded, update):
             for s in range(seqs):
-                q = g * seqs + s
-                wide_key = jnp.broadcast_to(keys_t[:, q : q + 1], (head, head))
+                q = h * share + g * seqs + s
+                near = g * seqs + s
+                wide_key = jnp.broadcast_to(keys_t[:, near : near + 1], (head, head))
                 for j, v in enumerate(owned):
                     cols = slice(j * head, (j + 1) * head)
                     new_state[q, v] = (
                         new_state[q, v] * faded[s : s + 1, cols] + wide_key * update[s : s + 1, cols]
                     )
 
-        groups = own // seqs
+        groups = share // seqs
         ready = ask(0)
         for g in range(groups):
             later = ask(g + 1) if g + 1 < groups else None
@@ -478,115 +491,222 @@
 
         for j in range(repeat):
             cols = slice(j * head, (j + 1) * head)
-            one = readouts[:, :, cols].reshape(own, head)
+            one = readouts[:, :, cols].reshape(share, head)
             normed = one * lax.rsqrt(jnp.mean(one * one, axis=1, keepdims=True) + EPSILON)
-            mine[c, :, cols] = (normed * gain_out * gate[:, cols]).astype(BF16)
-        gather_g.start(c)
-        gathered[c, kv] = mine[c]
-
-    scatter_p.relay(0)
+            mine[index, :, cols] = (normed * gain_out * gate[:, cols]).astype(BF16)
+        gather_g.start(index)
+        gathered[index, kv] = mine[index]
+
+    def project_relay(h, c):
+        scatter_p.relay(h * chunks + c)
+
+    def project_start(h, c):
+        scatter_p.start(h * chunks + c)
+
+    def gated_forward(h, c):
+        gather_g.forward(h * chunks + c)
+
+    copies_of = {}
+
+    def send_tp(name, h, product, part, got, send_sem, recv_sem):
+        for t in range(n_tp):
+            part[h, t] = product[:, t * own_cols : (t + 1) * own_cols].astype(BF16)
+        copies = scatter_copies("tp", n_tp, part.at[h], got.at[h], send_sem.at[h], recv_sem.at[h])
+        start(copies)
+        copies_of[name, h] = copies
+
+    def sum_tp(name, h, part, got):
+        wait_recv(copies_of[name, h])
+        total = part[h, tp].astype(F32)
+        for slot in range(n_tp - 1):
+            total = total + got[h, slot].astype(F32)
+        return total
+
+    def out_project(h):
+        if h == 0:
+            loads[19].wait()
+        product = jnp.zeros((half_rows, wo_v.shape[1]), F32)
+        for c in range(chunks):
+            gather_g.wait(h * chunks + c)
+            product = product + jnp.dot(
+                gathered[h * chunks + c].reshape(half_rows, span),
+                wo_v[c * span : (c + 1) * span, :],
+                preferred_element_type=F32,
+            )
+        send_tp("mix", h, product, mix_part, mix_got, m_send, m_recv)
+
+    def mix(h):
+        total = sum_tp("mix", h, mix_part, mix_got)
+        before = jnp.concatenate(
+            [stream_v[z * own + h * share : z * own + (h + 1) * share, :] for z in range(n_kv)], axis=0
+        )
+        mixed_own = (before.astype(F32) + total).astype(BF16)
+        mixed[h] = mixed_own
+        copies = gather_copies("tp", n_tp, mixed.at[h], blocks.at[h], b_send.at[h], b_recv.at[h])
+        start(copies)
+        copies_of["block", h] = copies
+        blocks[h, tp] = mixed_own
+
+    mlp_row = gain_row(mgain_v)
+    piece = wu_v.shape[1] // pieces
+    corner = lax.broadcasted_iota(jnp.int32, (half_rows, half_rows), 0) == lax.broadcasted_iota(
+        jnp.int32, (half_rows, half_rows), 1
+    )
+
+    def up(h):
+        if h == 0:
+            loads[20].wait()
+        wait_recv(copies_of["block", h])
+        wide = jnp.concatenate([blocks[h, t] for t in range(n_tp)], axis=1).astype(F32)
+        scaled = (wide * mlp_row).astype(BF16)
+        for p in range(pieces):
+            product = jnp.dot(
+                scaled, wu_v[:, p * piece : (p + 1) * piece], preferred_element_type=F32
+            )
+            up_part[h * pieces + p] = product.reshape(n_kv, share, piece).astype(BF16)
+            scatter_u.start(h * pieces + p)
+        squares = jnp.sum(wide * wide, axis=1, keepdims=True)
+        flat = jnp.sum(jnp.where(corner, squares, 0.0), axis=0, keepdims=True)
+        sq_part[h, :, :half_rows] = jnp.broadcast_to(flat, (sq_part.shape[1], half_rows))
+        copies = gather_copies("kv", n_kv, sq_part.at[h], sq_got.at[h], q_send.at[h], q_recv.at[h])
+        start(copies)
+        copies_of["square", h] = copies
+        sq_got[h, kv, :, :half_rows] = sq_part[h, :, :half_rows]
+
+    def up_relay(h, p):
+        scatter_u.relay(h * pieces + p)
+
+    def activate(h, p):
+        index = h * pieces + p
+        active = jnp.maximum(scatter_u.total(index), 0.0)
+        active = (active * active).astype(BF16)
+        hidden[index] = active
+        gather_h.start(index)
+        hiddens[index, kv] = active
+
+    def hidden_forward(h, p):
+        gather_h.forward(h * pieces + p)
+
+    def down(h):
+        if h == 0:
+            loads[21].wait()
+        wait_recv(copies_of["square", h])
+        square_sum = sq_got[h, 0, :, :half_rows]
+        for z in range(1, n_kv):
+            square_sum = square_sum + sq_got[h, z, :, :half_rows]
+        spread = jnp.broadcast_to(
+            1.0 / (square_sum[0:1, :] / width + EPSILON), (half_rows, half_rows)
+        )
+        scale_squared = jnp.sum(jnp.where(corner, spread, 0.0), axis=1, keepdims=True)
+        product = jnp.zeros((half_rows, wdn_v.shape[1]), F32)
+        for p in range(pieces):
+            index = h * pieces + p
+            gather_h.wait(index)
+            product = product + jnp.dot(
+                hiddens[index].reshape(half_rows, piece),
+                wdn_v[p * piece : (p + 1) * piece, :],
+                preferred_element_type=F32,
+            )
+        send_tp("down", h, product * scale_squared, down_part, down_got, d_send, d_recv)
+
+    def finish(h):
+        total = sum_tp("down", h, down_part, down_got)
+        ended = (mixed[h].astype(F32) + total).astype(BF16)
+        for z in range(n_kv):
+            result[z * own + h * share : z * own + (h + 1) * share, :] = ended[
+                z * share : (z + 1) * share
+            ]
+
+    def settle_projections():
+        wait_send(stream_copies)
+        wait_send(extra_copies)
+        scatter_p.finish(halves * chunks)
+        gather_g.finish(halves * chunks)
+
+    def settle_hidden():
+        for name in ("mix", "block", "square"):
+            for h in range(halves):
+                wait_send(copies_of[name, h])
+        scatter_u.finish(halves * pieces)
+        gather_h.finish(halves * pieces)
+
+    last = chunks - 1
+    project_relay(0, 0)
     for c in range(chunks):
-        if c + 1 < chunks:
-            scatter_p.relay(c + 1)
-        heads(c)
-        if c == chunks - 2:
-            gather_g.forward(0)
-    for c in range(1 if chunks > 1 else 0, chunks):
-        gather_g.forward(c)
-
-    def reduce_tp(product, part, got, send_sem, recv_sem, meanwhile=None):
-        for t in range(n_tp):
-            part[t] = product[:, t * own_cols : (t + 1) * own_cols].astype(BF16)
-        copies = scatter_copies("tp", n_tp, part, got, send_sem, recv_sem)
-        start(copies)
-        if meanwhile is not None:
-            meanwhile()
-        wait_recv(copies)
-        total = part[tp].astype(F32)
-        for slot in range(n_tp - 1):
-            total = total + got[slot].astype(F32)
-        return total, copies
-
-    loads[19].wait()
-    product = jnp.zeros((rows, wo_v.shape[1]), F32)
-    for c in range(chunks):
-        gather_g.wait(c)
-        product = product + jnp.dot(
-            gathered[c].reshape(rows, span),
-            wo_v[c * span : (c + 1) * span, :],
-            preferred_element_type=F32,
-        )
-    total, mix_copies = reduce_tp(product, mix_part, mix_got, m_send, m_recv)
-    mixed_own = (stream_v[...].astype(F32) + total).astype(BF16)
-    mixed[...] = mixed_own
-    block_copies = gather_copies("tp", n_tp, mixed, blocks, b_send, b_recv)
-    start(block_copies)
-    blocks[tp] = mixed_own
-    mlp_row = gain_row(mgain_v)
-    loads[20].wait()
-    wait_recv(block_copies)
-    wide = jnp.concatenate([blocks[t] for t in range(n_tp)], axis=1).astype(F32)
-    scaled = (wide * mlp_row).astype(BF16)
-    piece = wu_v.shape[1] // pieces
-    for p in range(pieces):
-        product = jnp.dot(
-            scaled, wu_v[:, p * piece : (p + 1) * piece], preferred_element_type=F32
-        )
-        up_part[p] = product.reshape(n_kv, own, piece).astype(BF16)
-        scatter_u.start(p)
-    corner = lax.broadcasted_iota(jnp.int32, (rows, rows), 0) == lax.broadcasted_iota(
-        jnp.int32, (rows, rows), 1
-    )
-    squares = jnp.sum(wide * wide, axis=1, keepdims=True)
-    flat = jnp.sum(jnp.where(corner, squares, 0.0), axis=0, keepdims=True)
-    sq_part[...] = jnp.broadcast_to(flat, sq_part.shape)
-    square_copies = gather_copies("kv", n_kv, sq_part, sq_got, q_send, q_recv)
-    start(square_copies)
-    sq_got[kv] = sq_part[...]
-    scatter_p.finish(chunks)
-    gather_g.finish(chunks)
-
-    def activate(p):
-        active = jnp.maximum(scatter_u.total(p), 0.0)
-        active = (active * active).astype(BF16)
-        hidden[p] = active
-        gather_h.start(p)
-        hiddens[p, kv] = active
-
-    scatter_u.relay(0)
-    for p in range(pieces):
-        if p + 1 < pieces:
-            scatter_u.relay(p + 1)
-        activate(p)
-    for p in range(pieces):
-        gather_h.forward(p)
-    loads[21].wait()
-    wait_recv(square_copies)
-    square_sum = sq_got[0]
-    for z in range(1, n_kv):
-        square_sum = square_sum + sq_got[z]
-    spread = jnp.broadcast_to(1.0 / (square_sum[0:1, :] / width + EPSILON), (rows, rows))
-    scale_squared = jnp.sum(jnp.where(corner, spread, 0.0), axis=1, keepdims=True)
-    product = jnp.zeros((rows, wdn_v.shape[1]), F32)
-    for p in range(pieces):
-        gather_h.wait(p)
-        product = product + jnp.dot(
-            hiddens[p].reshape(rows, piece),
-            wdn_v[p * piece : (p + 1) * piece, :],
-            preferred_element_type=F32,
-        )
-
-    def settle():
-        for copies in (stream_copies, extra_copies, mix_copies, block_copies, square_copies):
-            wait_send(copies)
-        scatter_u.finish(pieces)
-        gather_h.finish(pieces)
-
-    total, down_copies = reduce_tp(
-        product * scale_squared, down_part, down_got, d_send, d_recv, settle
-    )
-    result[...] = (mixed[...].astype(F32) + total).astype(BF16)
-    wait_send(down_copies)
+        if c < last:
+            project_relay(0, c + 1)
+        heads(0, c)
+        if halves > 1:
+            project_start(1, c)
+    if halves == 1:
+        for c in range(chunks):
+            gated_forward(0, c)
+        out_project(0)
+        mix(0)
+        settle_projections()
+        up(0)
+        for p in range(pieces):
+            up_relay(0, p)
+            activate(0, p)
+        for p in range(pieces):
+            hidden_forward(0, p)
+        down(0)
+    else:
+        project_relay(1, 0)
+        gated_forward(0, 0)
+        for c in range(chunks):
+            if c < last:
+                project_relay(1, c + 1)
+            heads(1, c)
+            if c + 1 < last:
+                gated_forward(0, c + 1)
+            if c == last - 1:
+                gated_forward(0, last)
+                out_project(0)
+        gated_forward(1, 0)
+        mix(0)
+        for c in range(1, chunks):
+            gated_forward(1, c)
+        out_project(1)
+        settle_projections()
+        up(0)
+        mix(1)
+        up_relay(0, 0)
+        up(1)
+        for p in range(1, pieces):
+            up_relay(0, p)
+        for p in range(pieces):
+            activate(0, p)
+        for p in range(pieces):
+            up_relay(1, p)
+        for p in range(pieces):
+            hidden_forward(0, p)
+        for p in range(pieces):
+            activate(1, p)
+        down(0)
+        for p in range(pieces):
+            hidden_forward(1, p)
+        finish(0)
+        down(1)
+    settle_hidden()
+    finish(halves - 1)
+    for h in range(halves):
+        wait_send(copies_of["down", h])
+
+
+def store_kernel(result_v, state_v, result, state, sems):
+    parts = sems.shape[0] - 1
+    each = state_v.shape[0] // parts
+    copies = [
+        pltpu.make_async_copy(
+            state_v.at[i * each : (i + 1) * each], state.at[i * each : (i + 1) * each], sems.at[i]
+        )
+        for i in range(parts)
+    ]
+    copies.append(pltpu.make_async_copy(result_v, result, sems.at[parts]))
+    start(copies)
+    for copy in copies:
+        copy.wait()
 
 
 def on_device(
@@ -609,9 +729,14 @@
     span = repeat * head
     field = 2 * head + 2 * span
     units = w_up.shape[1]
-    pieces = 4
+    seqs = min(8, own)
+    halves = 2 if own % (4 * seqs) == 0 else 1
+    share = own // halves
+    half_rows = n_kv * share
+    pieces = 4 // halves
     piece = units // pieces
-    seqs = min(8, own)
+    ids = halves * chunks
+    shares = halves * pieces
     vmem = pl.BlockSpec(memory_space=pltpu.VMEM)
     hbm = pl.BlockSpec(memory_space=pltpu.HBM)
     dma = pltpu.SemaphoreType.DMA
@@ -628,7 +753,7 @@
         return pltpu.VMEM(dims, dtype)
 
     result, new_state = pl.pallas_call(
-        functools.partial(layer_kernel, n_kv, n_tp, width, head, repeat, chunks, pieces),
+        functools.partial(layer_kernel, n_kv, n_tp, width, head, repeat, chunks, pieces, halves),
         out_shape=(
             pltpu.VMEM((rows, own_cols), BF16),
             pltpu.VMEM(delta_state.shape, F32),
@@ -649,28 +774,28 @@
             buffer(*gain_shape, dtype=F32), buffer(8, LANES, dtype=F32),
             buffer(n_tp, rows, own_cols),
             buffer(n_kv, own, LANES, dtype=F32), buffer(n_kv - 1, own, LANES, dtype=F32),
-            buffer(chunks, n_kv, own, field), buffer(chunks, n_kv - 1, own, field),
-            buffer(chunks, own, field), buffer(chunks, own, field),
-            buffer(own // seqs, seqs, span, dtype=F32),
-            buffer(chunks, own, span), buffer(chunks, n_kv, own, span),
-            buffer(n_tp, rows, own_cols), buffer(n_tp - 1, rows, own_cols),
-            buffer(rows, own_cols), buffer(n_tp, rows, own_cols),
-            buffer(8, rows, dtype=F32), buffer(n_kv, 8, rows, dtype=F32),
-            buffer(pieces, n_kv, own, piece), buffer(pieces, n_kv - 1, own, piece),
-            buffer(pieces, own, piece), buffer(pieces, own, piece),
-            buffer(pieces, own, piece), buffer(pieces, n_kv, own, piece),
-            buffer(n_tp, rows, own_cols), buffer(n_tp - 1, rows, own_cols),
+            buffer(ids, n_kv, share, field), buffer(ids, n_kv - 1, share, field),
+            buffer(ids, share, field), buffer(ids, share, field),
+            buffer(share // seqs, seqs, span, dtype=F32),
+            buffer(ids, share, span), buffer(ids, n_kv, share, span),
+            buffer(halves, n_tp, half_rows, own_cols), buffer(halves, n_tp - 1, half_rows, own_cols),
+            buffer(halves, half_rows, own_cols), buffer(halves, n_tp, half_rows, own_cols),
+            buffer(halves, 8, rows, dtype=F32), buffer(halves, n_kv, 8, rows, dtype=F32),
+            buffer(shares, n_kv, share, piece), buffer(shares, n_kv - 1, share, piece),
+            buffer(shares, share, piece), buffer(shares, share, piece),
+            buffer(shares, share, piece), buffer(shares, n_kv, share, piece),
+            buffer(halves, n_tp, half_rows, own_cols), buffer(halves, n_tp - 1, half_rows, own_cols),
             dma((22,)), dma((chunks,)),
             dma((n_tp - 1,)), dma((n_tp - 1,)),
             dma((n_kv - 1,)), dma((n_kv - 1,)),
-            dma((chunks, n_kv - 1)), dma((chunks, n_kv - 1)), dma((chunks,)),
-            dma((chunks, n_kv - 1)), dma((chunks, n_kv - 1)), dma((chunks, n_kv)),
-            dma((n_tp - 1,)), dma((n_tp - 1,)),
-            dma((n_tp - 1,)), dma((n_tp - 1,)),
-            dma((n_kv - 1,)), dma((n_kv - 1,)),
-            dma((pieces, n_kv - 1)), dma((pieces, n_kv - 1)), dma((pieces,)),
-            dma((pieces, n_kv - 1)), dma((pieces, n_kv - 1)), dma((pieces, n_kv)),
-            dma((n_tp - 1,)), dma((n_tp - 1,)),
+            dma((ids, n_kv - 1)), dma((ids, n_kv - 1)), dma((ids,)),
+            dma((ids, n_kv - 1)), dma((ids, n_kv - 1)), dma((ids, n_kv)),
+            dma((halves, n_tp - 1)), dma((halves, n_tp - 1)),
+            dma((halves, n_tp - 1)), dma((halves, n_tp - 1)),
+            dma((halves, n_kv - 1)), dma((halves, n_kv - 1)),
+            dma((shares, n_kv - 1)), dma((shares, n_kv - 1)), dma((shares,)),
+            dma((shares, n_kv - 1)), dma((shares, n_kv - 1)), dma((shares, n_kv)),
+            dma((halves, n_tp - 1)), dma((halves, n_tp - 1)),
         ],
         compiler_params=pltpu.CompilerParams(
             collective_id=0, has_side_effects=True,
@@ -678,7 +803,18 @@
         ),
         name="layer",
     )(*ins)
-    return result, new_state
+    return pl.pallas_call(
+        store_kernel,
+        out_shape=(
+            jax.ShapeDtypeStruct(result.shape, BF16),
+            jax.ShapeDtypeStruct(delta_state.shape, F32),
+        ),
+        in_specs=[vmem, vmem],
+        out_specs=(hbm, hbm),
+        scratch_shapes=[dma((min(own, 8) + 1,))],
+        compiler_params=pltpu.CompilerParams(vmem_limit_bytes=2**20),
+        name="store",
+    )(result, new_state)
 
 
 def solution(mesh):

time: 72.7 us -> 69.9 us (0.961)
  local copies, waits for them, and re-layouts: 6.78 us -> 0 us
  Pallas kernels: 65.2 us -> 69.1 us
    unnamed x2 -> x0, local copies, waits for them, and re-layouts: 6.78 us -> none
    pallas_call x0 -> x1, Pallas kernels: none -> 5.94 us  [on_device(): pl.pallas_call(store_kernel, out_shape=(jax.ShapeDtypeStruct(result.shape...]
    pallas_call x1, Pallas kernels: 65.2 us -> 63.2 us  [on_device(): pl.pallas_call(functools.partial(layer_kernel, n_kv, n_tp, width, head, r...]
where the time goes in v3:
time: 69.9 us; the launch traced here: 69.8 us
  Pallas kernels  69.1 us (99%)
    pallas_call x1, Pallas kernels, on_device(): pl.pallas_call(functools.partial(layer_kernel, n_kv, n_tp, width, head, r...  63.2 us
    pallas_call x1, Pallas kernels, on_device(): pl.pallas_call(store_kernel, out_shape=(jax.ShapeDtypeStruct(result.shape...  5.94 us

profile of v3, /device:TPU:0, one launch (start us, length us, event | category | flops | bytes accessed | tf_op | source)
XLA Modules:
  0.0 69.8 jit_solution(10687241842494340680)
XLA Ops:
  0.6 63.2 %layer.1 = (bf16[128,128]{1,0:T(8,128)(2,1)S(1)}, f32[32,8,128,128]{3,2,1,0:T(8,128)S(1)}) custom-call(bf16[128,128]{1,0:T(8,128)(2,1)} %stream.1, s32[1,32]{1,0:T(1,128)} %bitcast.18, bf16[16,128]{1,0:T(8,128)(2,1)} %bitcast.16, f32[1,32]{1,0:T(1,128)} %bitcast.19, f32[1,32]{1,0:T(1,128)} %bitcast.20, bf16[1,128]{1,0:T(2,128)(2,1)} %bitcast.21, ...), custom_call_target="tpu_custom_call" | custom-call | tf_op jit(solution)/shard_map/layer/pallas_call | solution.py:755
  63.9 5.9 %store.1 = (bf16[128,128]{1,0:T(8,128)(2,1)}, f32[32,8,128,128]{3,2,1,0:T(8,128)}) custom-call(bf16[128,128]{1,0:T(8,128)(2,1)S(1)} %get-tuple-element.4.result_v, f32[32,8,128,128]{3,2,1,0:T(8,128)S(1)} %get-tuple-element.5.state_v), custom_call_target="tpu_custom_call" | custom-call | tf_op jit(solution)/shard_map/store/pallas_call | solution.py:806

commit v4 on v3

--- a/solution.py
+++ b/solution.py
@@ -344,16 +344,26 @@
 
     wide = jnp.concatenate([streams[t] for t in range(n_tp)], axis=1).astype(F32)
     scaled = (wide * norm_row).astype(BF16)
-    squares = jnp.sum(wide * wide, axis=1, keepdims=True)
-    loads[2].wait()
-    loads[3].wait()
-    beta = lax.dot_general(scaled, wb_v[...], CONTRACT_LAST, preferred_element_type=F32)
-    decay = lax.dot_general(scaled, wd_v[...], CONTRACT_LAST, preferred_element_type=F32)
-    part_e[...] = jnp.concatenate(
-        [beta, decay, jnp.broadcast_to(squares, (rows, LANES - 2 * heads_all))], axis=1
-    ).reshape(n_kv, own, LANES)
-    extra_copies = scatter_copies("kv", n_kv, part_e, got_e, e_send, e_recv)
-    start(extra_copies)
+
+    def extras():
+        loads[2].wait()
+        loads[3].wait()
+        beta = lax.dot_general(scaled, wb_v[...], CONTRACT_LAST, preferred_element_type=F32)
+        decay = lax.dot_general(scaled, wd_v[...], CONTRACT_LAST, preferred_element_type=F32)
+        squares = jnp.sum(wide * wide, axis=1, keepdims=True)
+        coarse = squares.astype(BF16)
+        fine = (squares - coarse.astype(F32)).astype(BF16)
+        spare = (LANES - 2 * heads_all) // 2
+        part_e[...] = jnp.concatenate(
+            [
+                beta.astype(BF16), decay.astype(BF16),
+                jnp.broadcast_to(coarse, (rows, spare)), jnp.broadcast_to(fine, (rows, spare)),
+            ],
+            axis=1,
+        ).reshape(n_kv, own, LANES)
+        copies = scatter_copies("kv", n_kv, part_e, got_e, e_send, e_recv)
+        start(copies)
+        return copies
 
     for copy in loads[4:8]:
         copy.wait()
@@ -369,6 +379,8 @@
                     :, h * share : (h + 1) * share
                 ]
         scatter_p.start(c)
+        if c == 0:
+            extra_copies = extras()
 
     for copy in loads[8:19]:
         copy.wait()
@@ -401,11 +413,14 @@
     shift = tp * heads_own
     own_params = pltpu.roll(params[...], lax.rem(LANES - shift, LANES), 1)
 
+    scatter_p.relay(0)
     wait_recv(extra_copies)
-    extra = part_e[kv]
+    extra = part_e[kv].astype(F32)
     for slot in range(n_kv - 1):
-        extra = extra + got_e[slot]
-    row_scale = lax.rsqrt(extra[:, 2 * heads_all : 2 * heads_all + 1] / width + EPSILON)
+        extra = extra + got_e[slot].astype(F32)
+    fine_at = heads_all + LANES // 2
+    square_sum = extra[:, 2 * heads_all : 2 * heads_all + 1] + extra[:, fine_at : fine_at + 1]
+    row_scale = lax.rsqrt(square_sum / width + EPSILON)
     terms = extra * row_scale
     own_beta = pltpu.roll(terms, lax.rem(LANES - shift, LANES), 1)
     own_decay = pltpu.roll(terms, lax.rem(2 * LANES - heads_all - shift, LANES), 1)
@@ -631,7 +646,6 @@
         gather_h.finish(halves * pieces)
 
     last = chunks - 1
-    project_relay(0, 0)
     for c in range(chunks):
         if c < last:
             project_relay(0, c + 1)
@@ -677,7 +691,6 @@
             up_relay(0, p)
         for p in range(pieces):
             activate(0, p)
-        for p in range(pieces):
             up_relay(1, p)
         for p in range(pieces):
             hidden_forward(0, p)
@@ -773,7 +786,7 @@
             buffer(*w_out.shape), buffer(*w_up.shape), buffer(*w_down.shape),
             buffer(*gain_shape, dtype=F32), buffer(8, LANES, dtype=F32),
             buffer(n_tp, rows, own_cols),
-            buffer(n_kv, own, LANES, dtype=F32), buffer(n_kv - 1, own, LANES, dtype=F32),
+            buffer(n_kv, own, LANES), buffer(n_kv - 1, own, LANES),
             buffer(ids, n_kv, share, field), buffer(ids, n_kv - 1, share, field),
             buffer(ids, share, field), buffer(ids, share, field),
             buffer(share // seqs, seqs, span, dtype=F32),

time: 69.9 us -> 68.5 us (0.980)
  Pallas kernels: 69.1 us -> 67.7 us
    pallas_call x1, Pallas kernels: 63.2 us -> 61.8 us  [on_device(): pl.pallas_call(functools.partial(layer_kernel, n_kv, n_tp, width, head, r...]
where the time goes in v4:
time: 68.5 us; the launch traced here: 68.4 us
  Pallas kernels  67.7 us (99%)
    pallas_call x1, Pallas kernels, on_device(): pl.pallas_call(functools.partial(layer_kernel, n_kv, n_tp, width, head, r...  61.8 us
    pallas_call x1, Pallas kernels, on_device(): pl.pallas_call(store_kernel, out_shape=(jax.ShapeDtypeStruct(result.shape...  5.94 us

profile of v4, /device:TPU:0, one launch (start us, length us, event | category | flops | bytes accessed | tf_op | source)
XLA Modules:
  0.0 68.4 jit_solution(10315030180797649386)
XLA Ops:
  0.6 61.8 %layer.1 = (bf16[128,128]{1,0:T(8,128)(2,1)S(1)}, f32[32,8,128,128]{3,2,1,0:T(8,128)S(1)}) custom-call(bf16[128,128]{1,0:T(8,128)(2,1)} %stream.1, s32[1,32]{1,0:T(1,128)} %bitcast.18, bf16[16,128]{1,0:T(8,128)(2,1)} %bitcast.16, f32[1,32]{1,0:T(1,128)} %bitcast.19, f32[1,32]{1,0:T(1,128)} %bitcast.20, bf16[1,128]{1,0:T(2,128)(2,1)} %bitcast.21, ...), custom_call_target="tpu_custom_call" | custom-call | tf_op jit(solution)/shard_map/layer/pallas_call | solution.py:768
  62.4 5.9 %store.1 = (bf16[128,128]{1,0:T(8,128)(2,1)}, f32[32,8,128,128]{3,2,1,0:T(8,128)}) custom-call(bf16[128,128]{1,0:T(8,128)(2,1)S(1)} %get-tuple-element.4.result_v, f32[32,8,128,128]{3,2,1,0:T(8,128)S(1)} %get-tuple-element.5.state_v), custom_call_target="tpu_custom_call" | custom-call | tf_op jit(solution)/shard_map/store/pallas_call | solution.py:819

commit v5 on v4

--- a/solution.py
+++ b/solution.py
@@ -180,7 +180,7 @@
         self.mine, self.everyone = mine, everyone
         self.send, self.recv, self.relay_send = send, recv, relay_send
         self.relays = size >= 3
-        self.direct = [c for c in range(mine.shape[0]) if c % group >= group - DIRECT_LAST]
+        self.direct = [c for c in range(mine.shape[0]) if c % group >= group - DIRECT_LAST or (group > 2 and c >= 2 * group - 2)]
 
     def copy(self, c, step):
         peer = lax.rem(self.me + step, self.size)

time: 68.5 us -> 68.2 us (level)
  no operation moved by 1% of the time
where the time goes in v5:
time: 68.2 us; the launch traced here: 68.1 us
  Pallas kernels  67.5 us (99%)
    pallas_call x1, Pallas kernels, on_device(): pl.pallas_call(functools.partial(layer_kernel, n_kv, n_tp, width, head, r...  61.5 us
    pallas_call x1, Pallas kernels, on_device(): pl.pallas_call(store_kernel, out_shape=(jax.ShapeDtypeStruct(result.shape...  5.94 us

profile of v5, /device:TPU:0, one launch (start us, length us, event | category | flops | bytes accessed | tf_op | source)
XLA Modules:
  0.0 68.1 jit_solution(11227105709311964859)
XLA Ops:
  0.6 61.5 %layer.1 = (bf16[128,128]{1,0:T(8,128)(2,1)S(1)}, f32[32,8,128,128]{3,2,1,0:T(8,128)S(1)}) custom-call(bf16[128,128]{1,0:T(8,128)(2,1)} %stream.1, s32[1,32]{1,0:T(1,128)} %bitcast.18, bf16[16,128]{1,0:T(8,128)(2,1)} %bitcast.16, f32[1,32]{1,0:T(1,128)} %bitcast.19, f32[1,32]{1,0:T(1,128)} %bitcast.20, bf16[1,128]{1,0:T(2,128)(2,1)} %bitcast.21, ...), custom_call_target="tpu_custom_call" | custom-call | tf_op jit(solution)/shard_map/layer/pallas_call | solution.py:768
  62.2 5.9 %store.1 = (bf16[128,128]{1,0:T(8,128)(2,1)}, f32[32,8,128,128]{3,2,1,0:T(8,128)}) custom-call(bf16[128,128]{1,0:T(8,128)(2,1)S(1)} %get-tuple-element.4.result_v, f32[32,8,128,128]{3,2,1,0:T(8,128)S(1)} %get-tuple-element.5.state_v), custom_call_target="tpu_custom_call" | custom-call | tf_op jit(solution)/shard_map/store/pallas_call | solution.py:819
